TPU v7x, 32 devices: a whole 2x2x4 slice. The times are simulated.
32 devices in a mesh: sp: 16 (over z, y, x), tp: 2 (over core).
Axes of the slice: x: 2, y: 2, z: 4, core: 2. Of those that a mesh axis runs over, the one named last changes fastest.
Arguments:
- tokens: bfloat16 [4096, 2048], P('sp'), may hold values from -6 to 6
- input_norm_gain: float32 [2048], replicated, may hold values from 0.1 to 1.9
- query_matrix: bfloat16 [2048, 1024], P('sp', 'tp'), may hold values from -0.125 to 0.125
- key_matrix: bfloat16 [2048, 1024], P('sp', 'tp'), may hold values from -0.125 to 0.125
- value_matrix: bfloat16 [2048, 1024], P('sp', 'tp'), may hold values from -0.125 to 0.125
- convolution_value_matrix: bfloat16 [2048, 2048], P('sp', 'tp'), may hold values from -0.125 to 0.125
- convolution_gate_matrix: bfloat16 [2048, 2048], P('sp', 'tp'), may hold values from -0.125 to 0.125
- decay_offset_channel: float32 [1024], P('tp'), may hold values from -16 to -2
- decay_first_matrix: bfloat16 [2048, 128], replicated, may hold values from -0.125 to 0.125
- decay_second_matrix: bfloat16 [128, 1024], P(None, 'tp'), may hold values from -0.59765625 to 0.59765625
- learning_rate_offset: float32 [1024], P('tp'), may hold values from -9 to 1
- learning_rate_first_matrix: bfloat16 [2048, 128], replicated, may hold values from -0.125 to 0.125
- learning_rate_second_matrix: bfloat16 [128, 1024], P(None, 'tp'), may hold values from -0.5 to 0.5
- forgetting_rate_factor: float32 [4096, 16], P('sp', 'tp'), may hold values from 0.39 to 2.53
- state_retention_share: float32 [4096, 16], P('sp', 'tp'), may hold values from 0.12 to 1
- per_head_norm_gain: float32 [1024], P('tp'), may hold values from 0.1 to 1.9
- convolution_filter_taps: float32 [31, 2048], P(None, 'tp'), may hold values from -81 to 81
- convolution_channel_gain: float32 [2048], P('tp'), may hold values from 0.1 to 1.9
- attention_output_matrix: bfloat16 [2048, 1024], P('sp', 'tp'), may hold values from -0.109375 to 0.109375
- convolution_output_matrix: bfloat16 [2048, 2048], P('sp', 'tp'), may hold values from -0.109375 to 0.109375
Outputs:
- mixed: bfloat16 [4096, 2048], P('sp')
All inputs are finite; a program needn't handle non-finite values.
Results may differ from a plain program's by a relative error of at most 0.014.
Values may be sent and summed in bfloat16 or wider, within the bound.
A program may use at most 128 MiB of HBM per device.

v0:
```python
import functools
import math

import jax
import jax.numpy as jnp
from jax import lax
from jax.experimental import pallas as pl
from jax.experimental.pallas import tpu as pltpu
from jax.sharding import PartitionSpec as P


MESH = pl.DeviceIdType.MESH
HIGHEST = lax.Precision.HIGHEST
RMS_EPSILON = 1e-06
GROUP_EPSILON = 0.00064
LAYER_EPSILON = 1e-05
UNIT_EPSILON = 1e-06
EXP_HALF = math.exp(-0.5)


def split(x):
    top = x.astype(jnp.bfloat16)
    return top, (x - top.astype(jnp.float32)).astype(jnp.bfloat16)


def dot3(left, right, dims=((1,), (0,))):
    (lh, ll), (rh, rl) = split(left), split(right)

    def one(p, q):
        return lax.dot_general(p, q, (dims, ((), ())), preferred_element_type=jnp.float32)

    return one(lh, rh) + (one(lh, rl) + one(ll, rh))


def dot3t(left, right):
    return dot3(left, right, ((1,), (1,)))


def exact(left, right):
    return jnp.dot(left, right, precision=HIGHEST, preferred_element_type=jnp.float32)


def column(values, index):
    lanes = lax.broadcasted_iota(jnp.int32, values.shape, 1)
    return jnp.sum(jnp.where(lanes == index, values, 0.0), axis=1, keepdims=True)


def delta_kernel(
    head_size, chunk, block,
    query_ref, key_ref, value_ref, decay_ref, rate_ref, factor_ref, share_ref,
    local_ref, carried_ref, pair_ref,
):
    rows, width = query_ref.shape
    pair = pl.program_id(0)
    per = width // head_size
    lane = lax.broadcasted_iota(jnp.int32, (1, width), 1)
    lane_head = lane // head_size
    row_w = lax.broadcasted_iota(jnp.int32, (width, width), 0)
    col_w = lax.broadcasted_iota(jnp.int32, (width, width), 1)
    same_head = (row_w // head_size) == (col_w // head_size)
    ones_head = jnp.where(same_head, 1.0, 0.0)
    row_b = lax.broadcasted_iota(jnp.int32, (block, block), 0)
    col_b = lax.broadcasted_iota(jnp.int32, (block, block), 1)
    same_chunk = (row_b // chunk) == (col_b // chunk)
    strict = same_chunk & (row_b > col_b)
    incl = same_chunk & (row_b >= col_b)
    sums = jnp.concatenate([jnp.where(incl, 1.0, 0.0), jnp.where(same_chunk, 1.0, 0.0)], axis=0)
    eye_b = jnp.where(row_b == col_b, 1.0, 0.0)

    factor, share = factor_ref[...], jnp.log(share_ref[...])
    factor_w = jnp.zeros((rows, width), jnp.float32)
    share_w = jnp.zeros((rows, width), jnp.float32)
    for h in range(per):
        factor_w = jnp.where(lane_head == h, column(factor, pair * per + h), factor_w)
        share_w = jnp.where(lane_head == h, column(share, pair * per + h), share_w)
    logdec = share_w - (EXP_HALF * jax.nn.sigmoid(decay_ref[...])) * factor_w
    learn = jax.nn.sigmoid(rate_ref[...])
    key = key_ref[...]
    unit = key * lax.rsqrt(exact(key * key, ones_head) + UNIT_EPSILON)

    blocks = []
    for start in range(0, rows, block):
        cut = slice(start, start + block)
        q, k, v, ld = query_ref[cut], key[cut], value_ref[cut], logdec[cut]
        er, wr = -unit[cut], unit[cut] * learn[cut]
        both = exact(sums, ld)
        gain, total = both[:block], both[block:]
        mid = 0.5 * total
        up, down, bup = jnp.exp(gain - mid), jnp.exp(mid - gain), jnp.exp(gain - ld - mid)
        ehat, qhat, what, khat = er * bup, q * up, wr * down, k * down
        right = jnp.concatenate([what, khat], axis=0)
        eh_full, q_full = er * jnp.exp(gain - ld), q * jnp.exp(gain)
        to_end = jnp.exp(total - gain)
        pulled = solved = local = query = None
        heads = []
        for h in range(per):
            left = jnp.where(lane_head == h, jnp.concatenate([ehat, qhat], axis=0), 0.0)
            grid = dot3t(left, right)
            ew = jnp.where(strict, grid[:block, :block], 0.0)
            ek = jnp.where(strict, grid[:block, block:], 0.0)
            rw = jnp.where(incl, grid[block:, :block], 0.0)
            rk = jnp.where(incl, grid[block:, block:], 0.0)
            size = 2
            off = (row_b // size == col_b // size) & (row_b > col_b)
            inv = eye_b + jnp.where(off, ew, 0.0)
            while size < chunk:
                off = (row_b // (2 * size) == col_b // (2 * size)) & (row_b // size > col_b // size)
                inv = inv + dot3(dot3(inv, jnp.where(off, ew, 0.0)), inv)
                size *= 2
            seen = dot3(jnp.concatenate([ek, rk], axis=0), v)
            both = dot3(inv, jnp.concatenate([seen[:block], eh_full], axis=1))
            read = dot3(rw, both)
            heads.append((both[:, :width], both[:, width:], read[:, :width] + seen[block:], read[:, width:]))
        merged = list(heads[0])
        for h in range(1, per):
            merged = [jnp.where(lane_head == h, new, old) for new, old in zip(heads[h], merged)]
        pulled, solved, local, query = merged
        blocks.append((pulled, solved, local, q_full + query, v, wr * to_end, k * to_end, jnp.exp(total)))

    state = jnp.concatenate([jnp.where(row_w == col_w, 1.0, 0.0), jnp.zeros((width, width), jnp.float32)], axis=0)
    across = ((0,), (0,))
    for number, (pulled, solved, local, query, v, wend, kend, gain) in enumerate(blocks):
        for first in range(0, block, chunk):
            cut = slice(first, first + chunk)
            place = slice(number * block + first, number * block + first + chunk)
            got = dot3t(query[cut], state)
            carried_ref[place] = got[:, :width]
            local_ref[place] = local[cut] + got[:, width:]
            step = jnp.where(same_head, dot3(solved[cut], wend[cut], across), 0.0)
            added = dot3(
                jnp.concatenate([pulled[cut], v[cut]], axis=0),
                jnp.concatenate([wend[cut], kend[cut]], axis=0),
                across,
            )
            added = jnp.where(same_head, added, 0.0)
            moved = state * gain[first : first + 1] + dot3(state, step)
            state = jnp.concatenate([moved[:width], moved[width:] + added], axis=0)
    pair_ref[0] = state


def finish_kernel(head_size, local_ref, carried_ref, state_ref, gain_ref, out_ref):
    width = local_ref.shape[1]
    row_w = lax.broadcasted_iota(jnp.int32, (width, width), 0)
    col_w = lax.broadcasted_iota(jnp.int32, (width, width), 1)
    same_head = (row_w // head_size) == (col_w // head_size)
    average = jnp.where(same_head, 1.0 / head_size, 0.0)
    y = local_ref[...] + dot3t(carried_ref[...], state_ref[0])
    centred = y - exact(y, average)
    variance = exact(centred * centred, average)
    out_ref[...] = (centred * lax.rsqrt(variance + GROUP_EPSILON) * gain_ref[...]).astype(jnp.bfloat16)


def from_behind(value, axis, steps):
    count = lax.axis_size(axis)
    initial, last = (max(0, -steps), min(count, count - steps))
    return lax.ppermute(value, axis, [(source, source + steps) for source in range(initial, last)])


def head_blocks(pairs, head_size):
    width = pairs.shape[-1]
    return jnp.stack(
        [pairs[:, a : a + head_size, a : a + head_size] for a in range(0, width, head_size)], axis=1
    )


def delta_rule(query, key, value, decay_pre, rate_pre, factor, share, gain):
    rows, channels = query.shape
    heads = factor.shape[1]
    head_size = channels // heads
    per = math.gcd(heads, max(1, 128 // head_size))
    width, pairs = per * head_size, heads // per
    block = math.gcd(rows, 128)
    chunk = math.gcd(block, 16)
    wide = pl.BlockSpec((rows, width), lambda i: (0, i))
    whole = pl.BlockSpec((rows, heads), lambda i: (0, 0))
    local, carried, pair = pl.pallas_call(
        functools.partial(delta_kernel, head_size, chunk, block),
        grid=(pairs,),
        in_specs=[wide] * 5 + [whole] * 2,
        out_specs=[wide, wide, pl.BlockSpec((1, 2 * width, width), lambda i: (i, 0, 0))],
        out_shape=[
            jax.ShapeDtypeStruct((rows, channels), jnp.float32),
            jax.ShapeDtypeStruct((rows, channels), jnp.float32),
            jax.ShapeDtypeStruct((pairs, 2 * width, width), jnp.float32),
        ],
        cost_estimate=pl.CostEstimate(
            flops=pairs * rows * width * width * 60, bytes_accessed=rows * channels * 32, transcendentals=rows * channels * 10
        ),
        name="delta_chunks",
    )(query, key, value, decay_pre, rate_pre, factor, share)

    phi, psi = head_blocks(pair[:, :width], head_size), head_blocks(pair[:, width:], head_size)
    both = jnp.concatenate([phi, psi], axis=-2).reshape(heads, 2 * head_size, head_size)
    count, place = lax.axis_size("sp"), lax.axis_index("sp")
    steps = 1
    while steps < count - 1:
        earlier = from_behind(both, "sp", steps)
        new = exact_mul("hcd,hde->hce", earlier, both[:, :head_size])
        new = new + jnp.concatenate([jnp.zeros_like(both[:, :head_size]), both[:, head_size:]], axis=1)
        both = jnp.where(place >= steps, new, both)
        steps *= 2
    state = from_behind(both[:, head_size:], "sp", 1).reshape(pairs, per, head_size, head_size)
    same = jnp.eye(per, dtype=jnp.float32)
    state = (state[:, :, :, None, :] * same[None, :, None, :, None]).reshape(pairs, width, width)
    return pl.pallas_call(
        functools.partial(finish_kernel, head_size),
        grid=(pairs,),
        in_specs=[wide, wide, pl.BlockSpec((1, width, width), lambda i: (i, 0, 0)), pl.BlockSpec((1, width), lambda i: (0, i))],
        out_specs=wide,
        out_shape=jax.ShapeDtypeStruct((rows, channels), jnp.bfloat16),
        name="delta_finish",
    )(local, carried, state, gain[None])


def exact_mul(form, left, right):
    return jnp.einsum(form, left, right, precision=HIGHEST)


def gather_kernel(axis, radices, number, *refs):
    ins, outs = refs[:number], refs[number : 2 * number]
    own_sem, far_send, far_recv, near_send, near_recv = refs[2 * number :]
    outer, middle, inner = radices
    me = lax.axis_index(axis)
    x, y, z = me % inner, (me // inner) % middle, me // (inner * middle)

    def index(z_at, y_at, x_at):
        return (z_at * middle + y_at) * inner + x_at

    far = [index((z + step) % outer, y, x) for step in range(1, outer)]
    near = {}
    if inner == 2:
        near["x"] = index(z, y, 1 - x)
    if middle == 2:
        near["y"] = index(z, 1 - y, x)
    barrier = pltpu.get_barrier_semaphore()
    peers = far + list(near.values())
    for peer in peers:
        pl.semaphore_signal(barrier, inc=1, device_id={axis: peer}, device_id_type=MESH)
    pl.semaphore_wait(barrier, len(peers))

    def far_copy(w, step, to, z_from):
        return pltpu.make_async_remote_copy(
            src_ref=ins[w],
            dst_ref=outs[w].at[z_from, y, x],
            send_sem=far_send.at[w, step],
            recv_sem=far_recv.at[w, step],
            device_id={axis: to},
            device_id_type=MESH,
        )

    own = [pltpu.make_async_copy(ins[w], outs[w].at[z, y, x], own_sem.at[w]) for w in range(number)]
    for w in range(number):
        own[w].start()
        for step in range(outer - 1):
            far_copy(w, step, far[step], z).start()

    def region(w, order, stage, from_y, from_x):
        if stage == 0:
            return outs[w].at[:, from_y, from_x]
        return outs[w].at[:, from_y] if order[0] == "x" else outs[w].at[:, :, from_x]

    def near_copy(w, order, stage, from_y, from_x):
        part = region(w, order, stage, from_y, from_x)
        return pltpu.make_async_remote_copy(
            src_ref=part,
            dst_ref=part,
            send_sem=near_send.at[w, stage],
            recv_sem=near_recv.at[w, stage],
            device_id={axis: near[order[stage]]},
            device_id_type=MESH,
        )

    def theirs(w, order, stage):
        from_y, from_x = (y, 1 - x) if order[stage] == "x" else (1 - y, x)
        return near_copy(w, order, stage, from_y, from_x)

    names = list(near)
    orders = [names if w % 2 == 0 else names[::-1] for w in range(number)]

    def advance(w, stage):
        if stage == 0:
            own[w].wait()
            for step in range(outer - 1):
                far_copy(w, step, far[step], (z + outer - step - 1) % outer).wait_recv()
        else:
            theirs(w, orders[w], stage - 1).wait_recv()
        if stage < len(names):
            near_copy(w, orders[w], stage, y, x).start()

    last = len(names)
    for tick in range(number + last):
        for stage in range(last, -1, -1):
            w = tick - stage
            if 0 <= w < number:
                advance(w, stage)
    for w in range(number):
        for step in range(outer - 1):
            far_copy(w, step, far[step], z).wait_send()
        for stage in range(last):
            near_copy(w, orders[w], stage, y, x).wait_send()


def gather_rows(arrays, axis):
    count, number = lax.axis_size(axis), len(arrays)
    inner = math.gcd(count, 2)
    middle = math.gcd(count // inner, 2)
    radices = (count // inner // middle, middle, inner)
    outs = pl.pallas_call(
        functools.partial(gather_kernel, axis, radices, number),
        in_specs=[pl.BlockSpec(memory_space=pltpu.VMEM)] * number,
        out_specs=[pl.BlockSpec(memory_space=pl.ANY)] * number,
        out_shape=[jax.ShapeDtypeStruct(radices + item.shape, item.dtype) for item in arrays],
        scratch_shapes=[
            pltpu.SemaphoreType.DMA((number,)),
            pltpu.SemaphoreType.DMA((number, max(1, radices[0] - 1))),
            pltpu.SemaphoreType.DMA((number, max(1, radices[0] - 1))),
            pltpu.SemaphoreType.DMA((number, 2)),
            pltpu.SemaphoreType.DMA((number, 2)),
        ],
        compiler_params=pltpu.CompilerParams(collective_id=0, has_side_effects=True),
        cost_estimate=pl.CostEstimate(
            flops=10**9, bytes_accessed=sum(item.size for item in arrays) * 2 * count, transcendentals=0
        ),
        name="gather_rows",
    )(*arrays)
    return [out.reshape((-1,) + item.shape[1:]) for out, item in zip(outs, arrays)]


def body(
    tokens,
    input_norm_gain,
    query_matrix,
    key_matrix,
    value_matrix,
    convolution_value_matrix,
    convolution_gate_matrix,
    decay_offset_channel,
    decay_first_matrix,
    decay_second_matrix,
    learning_rate_offset,
    learning_rate_first_matrix,
    learning_rate_second_matrix,
    forgetting_rate_factor,
    state_retention_share,
    per_head_norm_gain,
    convolution_filter_taps,
    convolution_channel_gain,
    attention_output_matrix,
    convolution_output_matrix,
):
    tok_rows = tokens.shape[0]
    widened = tokens.astype(jnp.float32)
    normed = (
        widened
        * lax.rsqrt(jnp.mean(widened * widened, axis=-1, keepdims=True) + RMS_EPSILON)
        * input_norm_gain
    ).astype(jnp.bfloat16)
    pieces = (
        *gather_rows((query_matrix, key_matrix, value_matrix), "sp"),
        lax.all_gather(convolution_value_matrix, "sp", axis=0, tiled=True),
        lax.all_gather(convolution_gate_matrix, "sp", axis=0, tiled=True),
    )
    query_proj, key_proj, value_proj, conv_value, conv_gate = tuple(
        (jnp.dot(normed, piece, preferred_element_type=jnp.float32) for piece in pieces)
    )
    decay_mid = jnp.tanh(
        jnp.dot(normed, decay_first_matrix, preferred_element_type=jnp.float32)
    ).astype(jnp.bfloat16)
    rate_mid = jnp.dot(
        normed, learning_rate_first_matrix, preferred_element_type=jnp.float32
    ).astype(jnp.bfloat16)
    decay_pre = decay_offset_channel + jnp.dot(
        decay_mid, decay_second_matrix, preferred_element_type=jnp.float32
    )
    rate_pre = learning_rate_offset + jnp.dot(
        rate_mid, learning_rate_second_matrix, preferred_element_type=jnp.float32
    )
    state_mixed = delta_rule(
        query_proj, key_proj, value_proj, decay_pre, rate_pre,
        forgetting_rate_factor, state_retention_share, per_head_norm_gain,
    )
    gated = (conv_value * jax.nn.sigmoid(conv_gate)).astype(jnp.bfloat16)
    span = convolution_filter_taps.shape[0]
    rim = from_behind(gated[tok_rows - (span - 1) :], "sp", 1)
    padded = jnp.concatenate([rim, gated], axis=0)
    filtered = jnp.zeros(gated.shape, jnp.float32)
    for offset in range(span):
        filtered = filtered + convolution_filter_taps[offset] * padded[offset : offset + tok_rows]
    total_sum, total_square = lax.psum(
        (jnp.sum(filtered, axis=-1), jnp.sum(filtered * filtered, axis=-1)), "tp"
    )
    conv_channels = filtered.shape[1] * lax.axis_size("tp")
    row_mean = total_sum / conv_channels
    deviation = filtered - row_mean[:, None]
    variance = total_square / conv_channels - row_mean * row_mean
    conv_mixed = jax.nn.silu(
        deviation * lax.rsqrt(variance + LAYER_EPSILON)[:, None] * convolution_channel_gain
    ).astype(jnp.bfloat16)
    contract_dims = (((1,), (1,)), ((), ()))
    pieces = lax.all_gather(
        (attention_output_matrix, convolution_output_matrix), "sp", axis=0, tiled=True
    )
    partial_out = lax.dot_general(
        state_mixed, pieces[0], contract_dims, preferred_element_type=jnp.float32
    ) + lax.dot_general(conv_mixed, pieces[1], contract_dims, preferred_element_type=jnp.float32)
    partial_out = partial_out.astype(jnp.bfloat16)
    if lax.axis_size("tp") != 2:
        return lax.psum(partial_out, "tp")
    other = lax.ppermute(partial_out, "tp", [(0, 1), (1, 0)])
    return (partial_out.astype(jnp.float32) + other.astype(jnp.float32)).astype(jnp.bfloat16)


def solution(mesh):
    return jax.shard_map(
        body,
        mesh=mesh,
        in_specs=(
            P("sp", None),
            P(),
            P("sp", "tp"),
            P("sp", "tp"),
            P("sp", "tp"),
            P("sp", "tp"),
            P("sp", "tp"),
            P("tp"),
            P(),
            P(None, "tp"),
            P("tp"),
            P(),
            P(None, "tp"),
            P("sp", "tp"),
            P("sp", "tp"),
            P("tp"),
            P(None, "tp"),
            P("tp"),
            P("sp", "tp"),
            P("sp", "tp"),
        ),
        out_specs=P("sp", None),
        check_vma=False,
    )
```

profile of v0, /device:TPU:0, one launch (start us, length us, event | category | flops | bytes accessed | tf_op | source)
XLA Modules:
  0.0 363.1 jit_solution(15472160627627974939)
XLA Ops:
  11.7 123.4 %gather_rows.1 = (bf16[4,2,2,128,512]{4,3,2,1,0:T(8,128)(2,1)}, bf16[4,2,2,128,512]{4,3,2,1,0:T(8,128)(2,1)}, bf16[4,2,2,128,512]{4,3,2,1,0:T(8,128)(2,1)}) custom-call(bf16[128,512]{1,0:T(8,128)(2,1)} %refs_0_.1, bf16[128,512]{1,0:T(8,128)(2,1)} %refs_1_.1, bf16[128,512]{1,0:T(8,128)(2,1)} %refs_2_.1), custom_call_target="tpu_custom_call" | custom-call | flops 1000000000 | bytes 6291456 | tf_op jit(solution)/shard_map/gather_rows/pallas_call | solution.py:308
  138.5 3.3 fusion.59.value_ref
  141.8 1.6 fusion.61.key_ref
  145.0 56.6 %delta_chunks.1 = (f32[256,512]{1,0:T(8,128)}, f32[256,512]{1,0:T(8,128)}, f32[4,256,128]{2,1,0:T(8,128)}) custom-call(f32[256,512]{1,0:T(8,128)} %fusion.63.query_ref, f32[256,512]{1,0:T(8,128)} %fusion.61.key_ref, f32[256,512]{1,0:T(8,128)} %fusion.59.value_ref, f32[256,512]{1,0:T(8,128)} %convolution_add_fusion.2.decay_ref, ...), custom_call_target="tpu_custom_call" | custom-call | flops 1006632960 | bytes 4194304 | tf_op jit(solution)/shard_map/delta_chunks/pallas_call | solution.py:176
  203.0 10.7 %collective-permute-start = (f32[8,128,64]{1,2,0:T(8,128)S(1)}, f32[8,128,64]{1,2,0:T(8,128)S(1)}, u32[]{:S(2)}, u32[]{:S(2)}) collective-permute-start(f32[8,128,64]{1,2,0:T(8,128)S(1)} %bitcast.61), channel_id=1, source_target_pairs={{0,2},{2,4},{4,6},{6,8},{8,10},{10,12},{12,14},{14,16},{16,18},{18... | collective-permute-start | bytes 786440 | tf_op jit(solution)/shard_map/ppermute | solution.py:156
  213.9 3.7 %collective-permute-done = f32[8,128,64]{1,2,0:T(8,128)S(1)} collective-permute-done((f32[8,128,64]{1,2,0:T(8,128)S(1)}, f32[8,128,64]{1,2,0:T(8,128)S(1)}, u32[]{:S(2)}, u32[]{:S(2)}) %collective-permute-start) | collective-permute-done | bytes 262176 | tf_op jit(solution)/shard_map/ppermute | solution.py:156
  218.0 4.5 %collective-permute-start.1 = (f32[8,128,64]{1,2,0:T(8,128)S(1)}, f32[8,128,64]{1,2,0:T(8,128)S(1)}, u32[]{:S(2)}, u32[]{:S(2)}) collective-permute-start(f32[8,128,64]{1,2,0:T(8,128)S(1)} %fusion.10), channel_id=1, source_target_pairs={{0,4},{2,6},{4,8},{6,10},{8,12},{10,14},{12,16},{14,18},{16,20},{1... | collective-permute-start | bytes 786440 | tf_op jit(solution)/shard_map/ppermute | solution.py:156
  222.6 6.8 %collective-permute-done.1 = f32[8,128,64]{1,2,0:T(8,128)S(1)} collective-permute-done((f32[8,128,64]{1,2,0:T(8,128)S(1)}, f32[8,128,64]{1,2,0:T(8,128)S(1)}, u32[]{:S(2)}, u32[]{:S(2)}) %collective-permute-start.1) | collective-permute-done | bytes 262176 | tf_op jit(solution)/shard_map/ppermute | solution.py:156
  229.8 41.5 %collective-permute-start.2 = (f32[8,128,64]{1,2,0:T(8,128)S(1)}, f32[8,128,64]{1,2,0:T(8,128)S(1)}, u32[]{:S(2)}, u32[]{:S(2)}) collective-permute-start(f32[8,128,64]{1,2,0:T(8,128)S(1)} %fusion.9), channel_id=1, source_target_pairs={{0,8},{2,10},{4,12},{6,14},{8,16},{10,18},{12,20},{14,22},{16,24},... | collective-permute-start | bytes 786440 | tf_op jit(solution)/shard_map/ppermute | solution.py:156
  271.4 4.0 %collective-permute-done.2 = f32[8,128,64]{1,2,0:T(8,128)S(1)} collective-permute-done((f32[8,128,64]{1,2,0:T(8,128)S(1)}, f32[8,128,64]{1,2,0:T(8,128)S(1)}, u32[]{:S(2)}, u32[]{:S(2)}) %collective-permute-start.2) | collective-permute-done | bytes 262176 | tf_op jit(solution)/shard_map/ppermute | solution.py:156
  275.8 18.7 %collective-permute-start.3 = (f32[8,128,64]{1,2,0:T(8,128)S(1)}, f32[8,128,64]{1,2,0:T(8,128)S(1)}, u32[]{:S(2)}, u32[]{:S(2)}) collective-permute-start(f32[8,128,64]{1,2,0:T(8,128)S(1)} %fusion.8), channel_id=1, source_target_pairs={{0,16},{2,18},{4,20},{6,22},{8,24},{10,26},{12,28},{14,30},{1,17},... | collective-permute-start | bytes 786440 | tf_op jit(solution)/shard_map/ppermute | solution.py:156
  295.0 4.4 %collective-permute-done.3 = f32[8,128,64]{1,2,0:T(8,128)S(1)} collective-permute-done((f32[8,128,64]{1,2,0:T(8,128)S(1)}, f32[8,128,64]{1,2,0:T(8,128)S(1)}, u32[]{:S(2)}, u32[]{:S(2)}) %collective-permute-start.3) | collective-permute-done | bytes 262176 | tf_op jit(solution)/shard_map/ppermute | solution.py:156
  299.9 5.5 %collective-permute-start.4 = (f32[8,64,64]{1,2,0:T(8,128)S(1)}, f32[8,64,64]{1,2,0:T(8,128)S(1)}, u32[]{:S(2)}, u32[]{:S(2)}) collective-permute-start(f32[8,64,64]{1,2,0:T(8,128)S(1)} %fusion.46), channel_id=1, source_target_pairs={{0,2},{2,4},{4,6},{6,8},{8,10},{10,12},{12,14},{14,16},{16,18},{18... | collective-permute-start | bytes 393224 | tf_op jit(solution)/shard_map/ppermute | solution.py:156
  305.5 3.8 %collective-permute-done.4 = f32[8,64,64]{1,2,0:T(8,128)S(1)} collective-permute-done((f32[8,64,64]{1,2,0:T(8,128)S(1)}, f32[8,64,64]{1,2,0:T(8,128)S(1)}, u32[]{:S(2)}, u32[]{:S(2)}) %collective-permute-start.4) | collective-permute-done | bytes 131104 | tf_op jit(solution)/shard_map/ppermute | solution.py:156
  309.9 4.6 %fusion.6 = f32[256,1024]{1,0:T(8,128)} fusion(bf16[2048,1024]{1,0:T(8,128)(2,1)} %all-gather.9.cloned.1.call-done, bf16[256,2048]{1,0:T(8,128)(2,1)S(1)} %copy-done.1, f32[2048]{0:T(1024)S(1)} %copy-done.7, f32[256]{0:T(256)S(1)} %add_rsqrt_fusion.1), kind=kOutput, calls=%fused_computation.41 | convolution fusion | flops 1076625408 | bytes 6300672 | tf_op jit(solution)/shard_map/dot_general | solution.py:364
  314.5 3.8 %fusion.7 = bf16[256,1024]{1,0:T(8,128)(2,1)S(1)} fusion(f32[256,1024]{1,0:T(8,128)} %fusion.6, bf16[2048,1024]{1,0:T(8,128)(2,1)} %all-gather.7.cloned.1.call-done, bf16[256,2048]{1,0:T(8,128)(2,1)S(1)} %copy-done.1, f32[2048]{0:T(1024)S(1)} %copy-done.7, f32[256]{0:T(256)S(1)} %add_rsqrt_fusion.1), kind=kOutput, calls=%fused_computation.42 | convolution fusion | flops 1076363264 | bytes 6824960 | tf_op jit(solution)/shard_map/dot_general | solution.py:364
  318.4 4.4 %collective-permute-start.5 = (bf16[30,1024]{1,0:T(8,128)(2,1)S(1)}, bf16[30,1024]{1,0:T(8,128)(2,1)S(1)}, u32[]{:S(2)}, u32[]{:S(2)}) collective-permute-start(bf16[30,1024]{1,0:T(8,128)(2,1)S(1)} %slice.316), channel_id=1, source_target_pairs={{0,2},{2,4},{4,6},{6,8},{8,10},{10,12},{12,14},{14,16},{16,18},{18... | collective-permute-start | bytes 184328 | tf_op jit(solution)/shard_map/ppermute | solution.py:156
  323.5 5.2 %delta_finish.1 = bf16[256,512]{1,0:T(8,128)(2,1)} custom-call(f32[256,512]{1,0:T(8,128)} %get-tuple-element.14.local_ref, f32[256,512]{1,0:T(8,128)} %get-tuple-element.15.carried_ref, f32[4,128,128]{2,1,0:T(8,128)} %broadcast_multiply_fusion.state_ref, f32[1,512]{1,0:T(1,128)} %bitcast.96), custom_call_target="tpu_custom_call" | custom-call | tf_op jit(solution)/shard_map/delta_finish/pallas_call | solution.py:205
  328.7 6.1 %fusion.65 = (f32[256]{0:T(256)S(1)}, f32[256]{0:T(256)S(1)}, f32[256,1024]{1,0:T(8,128)}) fusion(bf16[256,1024]{1,0:T(8,128)(2,1)S(1)} %fusion.7, f32[1024]{0:T(1024)S(1)} %bitcast.94, bf16[30,1024]{1,0:T(8,128)(2,1)S(1)} %collective-permute-done.5, f32[1024]{0:T(1024)S(1)} %bitcast.95, f32[1024]{0:T(1024)S(1)} %bitcast.66, f32[1024]{0:T(1024)S(1)} %bitcast.67, ...), kind=kLoop, calls=%fused_computation.121 | loop fusion | flops 48496128 | bytes 1763328 | tf_op jit(solution)/shard_map/reduce_sum | solution.py:390
  334.7 2.4 all-reduce.4
  337.2 4.1 %fusion.12 = f32[256,2048]{1,0:T(8,128)S(1)} fusion(bf16[2048,1024]{1,0:T(8,128)(2,1)} %all-gather.11.cloned.1.call-done, f32[256,1024]{1,0:T(8,128)} %get-tuple-element.21, f32[1024]{0:T(1024)S(1)} %copy-done.8, f32[256]{0:T(256)S(1)} %get-tuple-element.58, f32[256]{0:T(256)S(1)} %get-tuple-element.57), kind=kOutput, calls=%fused_computation.57 | convolution fusion | flops 1075838976 | bytes 7346176 | tf_op jit(solution)/shard_map/dot_general | solution.py:405
  341.3 8.8 %all-gather.5.cloned.1.call-done = bf16[2048,512]{1,0:T(8,128)(2,1)} async-done(((bf16[128,512]{1,0:T(8,128)(2,1)}), bf16[2048,512]{1,0:T(8,128)(2,1)}) %all-gather.5.cloned.1.call-update) | async-done | bytes 2097168 | tf_op jit(solution)/shard_map/all_gather | solution.py:400
  350.1 2.3 fusion
  352.5 2.6 collective-permute-done.6
  (70 shorter events, 16.8 us)
Async XLA Ops:
  6.5 128.9 %copy-start = (bf16[2048,128]{1,0:T(8,128)(2,1)S(1)}, bf16[2048,128]{1,0:T(8,128)(2,1)}, u32[]{:S(2)}) copy-start(bf16[2048,128]{1,0:T(8,128)(2,1)} %param.31) | copy-start | bytes 1572868
  6.5 303.4 %all-gather.9.cloned.1.call-start = ((), (), s32[]{:S(2)}) async-start(), calls=%async_computation.2 | async-start | bytes 4456448 | tf_op jit(solution)/shard_map/all_gather | solution.py:361
  7.3 307.2 %all-gather.7.cloned.1.call-start = ((), (), s32[]{:S(2)}) async-start(), calls=%async_computation.1 | async-start | bytes 4456448 | tf_op jit(solution)/shard_map/all_gather | solution.py:360
  8.0 127.1 %copy-start.1 = (bf16[256,2048]{1,0:T(8,128)(2,1)S(1)}, bf16[256,2048]{1,0:T(8,128)(2,1)}, u32[]{:S(2)}) copy-start(bf16[256,2048]{1,0:T(8,128)(2,1)} %param.20) | copy-start | bytes 3145732
  8.0 329.2 %all-gather.11.cloned.1.call-start = ((), (), s32[]{:S(2)}) async-start(), calls=%async_computation.3 | async-start | bytes 4456448 | tf_op jit(solution)/shard_map/all_gather | solution.py:400
  8.8 341.4 %all-gather.5.cloned.1.call-start = ((), (), s32[]{:S(2)}) async-start(), calls=%async_computation | async-start | bytes 2228224 | tf_op jit(solution)/shard_map/all_gather | solution.py:400
  11.7 123.7 %copy-start.5 = (bf16[128,512]{1,0:T(8,128)(2,1)S(1)}, bf16[128,512]{1,0:T(8,128)(2,1)}, u32[]{:S(2)}) copy-start(bf16[128,512]{1,0:T(8,128)(2,1)} %param.32) | copy-start | bytes 393220
  11.7 123.8 %copy-start.7 = (f32[2048]{0:T(1024)S(1)}, f32[2048]{0:T(1024)}, u32[]{:S(2)}) copy-start(f32[2048]{0:T(1024)} %param.21) | copy-start | bytes 24580
  11.7 123.8 %copy-start.9 = (f32[512]{0:T(512)S(1)}, f32[512]{0:T(512)}, u32[]{:S(2)}) copy-start(f32[512]{0:T(512)} %param.30) | copy-start | bytes 6148
  135.1 1.8 copy-start.4
  135.2 1.8 copy-start.6
  135.2 1.8 copy-start.10
  138.5 3.3 copy-start.12
  141.8 1.6 copy-start.11
  203.0 14.6 %collective-permute-start = (f32[8,128,64]{1,2,0:T(8,128)S(1)}, f32[8,128,64]{1,2,0:T(8,128)S(1)}, u32[]{:S(2)}, u32[]{:S(2)}) collective-permute-start(f32[8,128,64]{1,2,0:T(8,128)S(1)} %bitcast.61), channel_id=1, source_target_pairs={{0,2},{2,4},{4,6},{6,8},{8,10},{10,12},{12,14},{14,16},{16,18},{18... | collective-permute-start | bytes 786440 | tf_op jit(solution)/shard_map/ppermute | solution.py:156
  213.9 80.7 %copy-start.3 = (f32[31,1024]{1,0:T(8,128)S(1)}, f32[31,1024]{1,0:T(8,128)}, u32[]{:S(2)}) copy-start(f32[31,1024]{1,0:T(8,128)} %param.36) | copy-start | bytes 380932
  218.0 11.4 %collective-permute-start.1 = (f32[8,128,64]{1,2,0:T(8,128)S(1)}, f32[8,128,64]{1,2,0:T(8,128)S(1)}, u32[]{:S(2)}, u32[]{:S(2)}) collective-permute-start(f32[8,128,64]{1,2,0:T(8,128)S(1)} %fusion.10), channel_id=1, source_target_pairs={{0,4},{2,6},{4,8},{6,10},{8,12},{10,14},{12,16},{14,18},{16,20},{1... | collective-permute-start | bytes 786440 | tf_op jit(solution)/shard_map/ppermute | solution.py:156
  229.8 45.6 %collective-permute-start.2 = (f32[8,128,64]{1,2,0:T(8,128)S(1)}, f32[8,128,64]{1,2,0:T(8,128)S(1)}, u32[]{:S(2)}, u32[]{:S(2)}) collective-permute-start(f32[8,128,64]{1,2,0:T(8,128)S(1)} %fusion.9), channel_id=1, source_target_pairs={{0,8},{2,10},{4,12},{6,14},{8,16},{10,18},{12,20},{14,22},{16,24},... | collective-permute-start | bytes 786440 | tf_op jit(solution)/shard_map/ppermute | solution.py:156
  275.8 23.6 %collective-permute-start.3 = (f32[8,128,64]{1,2,0:T(8,128)S(1)}, f32[8,128,64]{1,2,0:T(8,128)S(1)}, u32[]{:S(2)}, u32[]{:S(2)}) collective-permute-start(f32[8,128,64]{1,2,0:T(8,128)S(1)} %fusion.8), channel_id=1, source_target_pairs={{0,16},{2,18},{4,20},{6,22},{8,24},{10,26},{12,28},{14,30},{1,17},... | collective-permute-start | bytes 786440 | tf_op jit(solution)/shard_map/ppermute | solution.py:156
  299.9 9.4 %collective-permute-start.4 = (f32[8,64,64]{1,2,0:T(8,128)S(1)}, f32[8,64,64]{1,2,0:T(8,128)S(1)}, u32[]{:S(2)}, u32[]{:S(2)}) collective-permute-start(f32[8,64,64]{1,2,0:T(8,128)S(1)} %fusion.46), channel_id=1, source_target_pairs={{0,2},{2,4},{4,6},{6,8},{8,10},{10,12},{12,14},{14,16},{16,18},{18... | collective-permute-start | bytes 393224 | tf_op jit(solution)/shard_map/ppermute | solution.py:156
  318.3 18.9 %copy-start.8 = (f32[1024]{0:T(1024)S(1)}, f32[1024]{0:T(1024)}, u32[]{:S(2)}) copy-start(f32[1024]{0:T(1024)} %param.37) | copy-start | bytes 12292
  318.4 10.3 %collective-permute-start.5 = (bf16[30,1024]{1,0:T(8,128)(2,1)S(1)}, bf16[30,1024]{1,0:T(8,128)(2,1)S(1)}, u32[]{:S(2)}, u32[]{:S(2)}) collective-permute-start(bf16[30,1024]{1,0:T(8,128)(2,1)S(1)} %slice.316), channel_id=1, source_target_pairs={{0,2},{2,4},{4,6},{6,8},{8,10},{10,12},{12,14},{14,16},{16,18},{18... | collective-permute-start | bytes 184328 | tf_op jit(solution)/shard_map/ppermute | solution.py:156
  337.2 12.9 %copy-start.2 = (bf16[256,512]{1,0:T(8,128)(2,1)S(1)}, bf16[256,512]{1,0:T(8,128)(2,1)}, u32[]{:S(2)}) copy-start(bf16[256,512]{1,0:T(8,128)(2,1)} %delta_finish.1) | copy-start | bytes 786436
  352.5 2.7 collective-permute-start.6
Sparse Core Ops, SparseCore 0:
  10.1 106.6 all-gather.8
  119.6 74.3 all-gather.6
  196.7 81.2 all-gather.10
  280.7 69.3 all-gather.4
where the time goes:
time: 364 us; the launch traced here: 363 us
  Pallas kernels  185 us (51%)
  starting transfers between devices  85.5 us (23%)
  waiting for transfers between devices  36.3 us (10%)
  matrix products  25.7 us (7%)
  between operations  13.5 us (4%)
  other arithmetic  8.63 us (2%)
  local copies, waits for them, and re-layouts  5.86 us (2%)
    pallas_call x1, Pallas kernels, gather_rows(): pl.pallas_call(functools.partial(gather_kernel, axis, radices, number), i...  123 us
    ppermute x6, starting transfers between devices, from_behind(): lax.ppermute(value, axis, [(source, source + steps) for source in range(i...  85.3 us
    pallas_call x1, Pallas kernels, delta_rule(): pl.pallas_call(functools.partial(delta_kernel, head_size, chunk, block),...  56.6 us
    ppermute x6, waiting for transfers between devices, from_behind(): lax.ppermute(value, axis, [(source, source + steps) for source in range(i...  22.7 us
    dot_general x5, matrix products, body(): jnp.dot(normed, piece, preferred_element_type=jnp.float32)  14.9 us
    all_gather x2, waiting for transfers between devices, body(): lax.all_gather((attention_output_matrix, convolution_output_matrix), 'sp'...  8.85 us
  transfers between devices with their start and end apart: 11, of which 7 were waited for; matrix products, arithmetic and copies ran while one was open for 10% of the time, Pallas kernels for 51%

commit v1 on v0

--- a/solution.py
+++ b/solution.py
@@ -51,8 +51,8 @@
     local_ref, carried_ref, pair_ref,
 ):
     rows, width = query_ref.shape
-    pair = pl.program_id(0)
     per = width // head_size
+    pair = 0 if factor_ref.shape[1] == per else pl.program_id(0)
     lane = lax.broadcasted_iota(jnp.int32, (1, width), 1)
     lane_head = lane // head_size
     row_w = lax.broadcasted_iota(jnp.int32, (width, width), 0)
@@ -300,7 +300,7 @@
             near_copy(w, orders[w], stage, y, x).wait_send()
 
 
-def gather_rows(arrays, axis):
+def gather_rows(arrays, axis, number_id=0):
     count, number = lax.axis_size(axis), len(arrays)
     inner = math.gcd(count, 2)
     middle = math.gcd(count // inner, 2)
@@ -317,7 +317,7 @@
             pltpu.SemaphoreType.DMA((number, 2)),
             pltpu.SemaphoreType.DMA((number, 2)),
         ],
-        compiler_params=pltpu.CompilerParams(collective_id=0, has_side_effects=True),
+        compiler_params=pltpu.CompilerParams(collective_id=number_id, has_side_effects=True),
         cost_estimate=pl.CostEstimate(
             flops=10**9, bytes_accessed=sum(item.size for item in arrays) * 2 * count, transcendentals=0
         ),
@@ -326,7 +326,7 @@
     return [out.reshape((-1,) + item.shape[1:]) for out, item in zip(outs, arrays)]
 
 
-def body(
+def plain_body(
     tokens,
     input_norm_gain,
     query_matrix,
@@ -410,6 +410,607 @@
     return (partial_out.astype(jnp.float32) + other.astype(jnp.float32)).astype(jnp.bfloat16)
 
 
+def radices_of(axis):
+    count = lax.axis_size(axis)
+    inner = math.gcd(count, 2)
+    middle = math.gcd(count // inner, 2)
+    return count // inner // middle, middle, inner
+
+
+def place_of(axis, radices):
+    outer, middle, inner = radices
+    me = lax.axis_index(axis)
+    return me // (inner * middle), (me // inner) % middle, me % inner
+
+
+def greet(devices):
+    barrier = pltpu.get_barrier_semaphore()
+    for device in devices:
+        pl.semaphore_signal(barrier, inc=1, device_id=device, device_id_type=MESH)
+    pl.semaphore_wait(barrier, len(devices))
+
+
+def spread_kernel(axis, pair_axis, radices, widths, placed, *refs):
+    number = len(widths)
+    tokens_ref, side_ref, ins = refs[0], refs[1], refs[2 : 2 + number]
+    kinds = 1 + max(out for out, _ in placed)
+    tokens_out, side_out, outs = refs[2 + number], refs[3 + number], refs[4 + number : 4 + number + kinds]
+    (own_sem, far_send, far_recv, near_send, near_recv, side_send, side_recv,
+     tok_send, tok_recv, sib_send, sib_recv) = refs[4 + number + kinds :]
+    outer, middle, inner = radices
+    z, y, x = place_of(axis, radices)
+    core = lax.axis_index(pair_axis)
+    half = tokens_ref.shape[0] // 2
+    mine, other = pl.ds(pl.multiple_of(core * half, half), half), pl.ds(pl.multiple_of((1 - core) * half, half), half)
+
+    def index(z_at, y_at, x_at):
+        return (z_at * middle + y_at) * inner + x_at
+
+    far = [(z + step) % outer for step in range(1, outer)]
+    near = {"x": index(z, y, 1 - x), "y": index(z, 1 - y, x)}
+    greet(
+        [{axis: index(at, y, x)} for at in far]
+        + [{axis: peer} for peer in near.values()]
+        + [{pair_axis: 1 - core}]
+    )
+
+    def part(w, at):
+        return ins[w].at[:, pl.ds(pl.multiple_of(at * widths[w], widths[w]), widths[w])]
+
+    def slot(w, *where):
+        out, offset = placed[w]
+        return outs[out].at[(*where, slice(None), pl.ds(offset, widths[w]))]
+
+    def far_copy(w, step, to, z_from):
+        return pltpu.make_async_remote_copy(
+            src_ref=part(w, to), dst_ref=slot(w, z_from, y, x),
+            send_sem=far_send.at[w, step], recv_sem=far_recv.at[w, step],
+            device_id={axis: index(to, y, x)}, device_id_type=MESH,
+        )
+
+    def side_copy(step, to, z_from):
+        return pltpu.make_async_remote_copy(
+            src_ref=side_ref, dst_ref=side_out.at[z_from],
+            send_sem=side_send.at[step], recv_sem=side_recv.at[step],
+            device_id={axis: index(to, y, x)}, device_id_type=MESH,
+        )
+
+    def near_copy(w, order, stage, y_at, x_at):
+        if stage == 0:
+            region = slot(w, slice(None), y_at, x_at)
+        elif order[0] == "x":
+            region = slot(w, slice(None), y_at, slice(None))
+        else:
+            region = slot(w, slice(None), slice(None), x_at)
+        return pltpu.make_async_remote_copy(
+            src_ref=region, dst_ref=region,
+            send_sem=near_send.at[w, stage], recv_sem=near_recv.at[w, stage],
+            device_id={axis: near[order[stage]]}, device_id_type=MESH,
+        )
+
+    def theirs(w, order, stage):
+        y_at, x_at = (y, 1 - x) if order[stage] == "x" else (1 - y, x)
+        return near_copy(w, order, stage, y_at, x_at)
+
+    def inside(at):
+        return (at >= 0) & (at < outer)
+
+    ways = (1, -1)
+
+    def token_copy(way, step, block, source):
+        return pltpu.make_async_remote_copy(
+            src_ref=source, dst_ref=tokens_out.at[block, mine],
+            send_sem=tok_send.at[way, step], recv_sem=tok_recv.at[way, step],
+            device_id={axis: index((z + ways[way] + outer) % outer, y, x)}, device_id_type=MESH,
+        )
+
+    def sibling_copy(way, step, block, rows):
+        return pltpu.make_async_remote_copy(
+            src_ref=tokens_out.at[block, rows], dst_ref=tokens_out.at[block, rows],
+            send_sem=sib_send.at[way, step], recv_sem=sib_recv.at[way, step],
+            device_id={pair_axis: 1 - core}, device_id_type=MESH,
+        )
+
+    def arrived(way, step):
+        return z - ways[way] * (step + 1)
+
+    def sends(way, step):
+        return inside(z + ways[way]) & inside(z - ways[way] * step)
+
+    own = [pltpu.make_async_copy(part(w, z), slot(w, z, y, x), own_sem.at[w]) for w in range(number)]
+    own.append(pltpu.make_async_copy(tokens_ref, tokens_out.at[z], own_sem.at[number]))
+    own.append(pltpu.make_async_copy(side_ref, side_out.at[z], own_sem.at[number + 1]))
+    for step in range(outer - 1):
+        side_copy(step, far[step], z).start()
+    for w in range(number):
+        own[w].start()
+        for step in range(outer - 1):
+            far_copy(w, step, far[step], z).start()
+    for way in range(2):
+        @pl.when(sends(way, 0))
+        def _():
+            token_copy(way, 0, z, tokens_ref.at[mine]).start()
+    own[number].start()
+    own[number + 1].start()
+
+    names = list(near)
+    orders = [names if w % 2 == 0 else names[::-1] for w in range(number)]
+
+    def advance(w, stage):
+        if stage == 0:
+            own[w].wait()
+            for step in range(outer - 1):
+                far_copy(w, step, far[step], (z + outer - step - 1) % outer).wait_recv()
+        else:
+            theirs(w, orders[w], stage - 1).wait_recv()
+        if stage < len(names):
+            near_copy(w, orders[w], stage, y, x).start()
+
+    def token_step(step):
+        for way in range(2):
+            block = arrived(way, step)
+            @pl.when(inside(block))
+            def _():
+                token_copy(way, step, block, tokens_out.at[block, mine]).wait_recv()
+                if step + 1 < outer - 1:
+                    @pl.when(sends(way, step + 1))
+                    def _():
+                        token_copy(way, step + 1, block, tokens_out.at[block, mine]).start()
+                sibling_copy(way, step, block, mine).start()
+
+    last = len(names)
+    steps = 0
+    for tick in range(number + last):
+        for stage in range(last, -1, -1):
+            w = tick - stage
+            if 0 <= w < number:
+                advance(w, stage)
+        if tick >= number - 1 and steps < outer - 1:
+            token_step(steps)
+            steps += 1
+    while steps < outer - 1:
+        token_step(steps)
+        steps += 1
+    own[number].wait()
+    own[number + 1].wait()
+    for step in range(outer - 1):
+        side_copy(step, far[step], (z + outer - step - 1) % outer).wait_recv()
+        side_copy(step, far[step], z).wait_send()
+    for step in range(outer - 1):
+        for way in range(2):
+            block = arrived(way, step)
+            @pl.when(inside(block))
+            def _():
+                sibling_copy(way, step, block, other).wait_recv()
+                sibling_copy(way, step, block, mine).wait_send()
+            @pl.when(sends(way, step))
+            def _():
+                token_copy(way, step, z - ways[way] * step, tokens_ref.at[mine]).wait_send()
+    for w in range(number):
+        for step in range(outer - 1):
+            far_copy(w, step, far[step], z).wait_send()
+        for stage in range(last):
+            near_copy(w, orders[w], stage, y, x).wait_send()
+
+
+def spread(normed, side, weights, groups, axis, pair_axis):
+    radices = radices_of(axis)
+    outer, number = radices[0], len(weights)
+    widths = [item.shape[1] // outer for item in weights]
+    placed, totals = [None] * number, []
+    for out, members in enumerate(groups):
+        offset = 0
+        for w in members:
+            placed[w] = (out, offset)
+            offset += widths[w]
+        totals.append(offset)
+    depth = weights[0].shape[0]
+    outs = pl.pallas_call(
+        functools.partial(spread_kernel, axis, pair_axis, radices, widths, placed),
+        in_specs=[pl.BlockSpec(memory_space=pltpu.VMEM)] * (2 + number),
+        out_specs=[pl.BlockSpec(memory_space=pl.ANY)] * (2 + len(groups)),
+        out_shape=[
+            jax.ShapeDtypeStruct((outer,) + normed.shape, normed.dtype),
+            jax.ShapeDtypeStruct((outer,) + side.shape, side.dtype),
+        ]
+        + [jax.ShapeDtypeStruct(radices + (depth, total), weights[0].dtype) for total in totals],
+        scratch_shapes=[
+            pltpu.SemaphoreType.DMA((number + 2,)),
+            pltpu.SemaphoreType.DMA((number, outer - 1)),
+            pltpu.SemaphoreType.DMA((number, outer - 1)),
+            pltpu.SemaphoreType.DMA((number, 2)),
+            pltpu.SemaphoreType.DMA((number, 2)),
+            pltpu.SemaphoreType.DMA((outer - 1,)),
+            pltpu.SemaphoreType.DMA((outer - 1,)),
+            pltpu.SemaphoreType.DMA((2, outer - 1)),
+            pltpu.SemaphoreType.DMA((2, outer - 1)),
+            pltpu.SemaphoreType.DMA((2, outer - 1)),
+            pltpu.SemaphoreType.DMA((2, outer - 1)),
+        ],
+        compiler_params=pltpu.CompilerParams(collective_id=0, has_side_effects=True),
+        cost_estimate=pl.CostEstimate(flops=10**9, bytes_accessed=2 * normed.size * 2 * outer, transcendentals=0),
+        name="spread_weights",
+    )(normed, side, *weights)
+    return outs[0], outs[1], [out.reshape(-1, total) for out, total in zip(outs[2:], totals)]
+
+
+def states_kernel(
+    axis, pair_axis, radices, head_size,
+    pair_ref, sums_ref, local_ref, carried_ref, gain_ref,
+    mixed_ref, totals_ref,
+    held, stats, own_sem, pair_send, pair_recv, stat_send, stat_recv,
+):
+    outer, middle, inner = radices
+    planes = middle * inner
+    z, y, x = place_of(axis, radices)
+    place = y * inner + x
+    core = lax.axis_index(pair_axis)
+    width = pair_ref.shape[-1]
+    rows = local_ref.shape[0] // outer
+    plane_peers = [(place + step) % planes for step in range(1, planes)]
+    cores = lax.axis_size(pair_axis)
+    lines = [(dz, dc) for dz in range(outer) for dc in range(cores) if dz or dc]
+
+    def line_device(dz, dc):
+        return {axis: ((z + dz) % outer) * planes + place, pair_axis: (core + dc) % cores}
+
+    greet([{axis: z * planes + peer} for peer in plane_peers] + [line_device(*line) for line in lines])
+
+    def pair_copy(step, p_from):
+        return pltpu.make_async_remote_copy(
+            src_ref=pair_ref, dst_ref=held.at[p_from],
+            send_sem=pair_send.at[step], recv_sem=pair_recv.at[step],
+            device_id={axis: z * planes + plane_peers[step]}, device_id_type=MESH,
+        )
+
+    def stat_copy(number, slot):
+        return pltpu.make_async_remote_copy(
+            src_ref=sums_ref, dst_ref=stats.at[slot],
+            send_sem=stat_send.at[number], recv_sem=stat_recv.at[number],
+            device_id=line_device(*lines[number]), device_id_type=MESH,
+        )
+
+    for step in range(planes - 1):
+        pair_copy(step, place).start()
+    for number in range(len(lines)):
+        stat_copy(number, number).start()
+    own = pltpu.make_async_copy(pair_ref, held.at[place], own_sem.at[0])
+    own.start()
+
+    for number in range(len(lines)):
+        stat_copy(number, number).wait_recv()
+    totals = sums_ref[...]
+    for number in range(len(lines)):
+        totals = totals + stats[number]
+    totals_ref[...] = totals
+
+    own.wait()
+    for step in range(planes - 1):
+        pair_copy(step, (place + planes - step - 1) % planes).wait_recv()
+
+    lane_head = lax.broadcasted_iota(jnp.int32, (1, width), 1) // head_size
+    row_w = lax.broadcasted_iota(jnp.int32, (width, width), 0)
+    col_w = lax.broadcasted_iota(jnp.int32, (width, width), 1)
+    average = jnp.where((row_w // head_size) == (col_w // head_size), 1.0 / head_size, 0.0)
+
+    def widen(compact):
+        return jnp.concatenate([jnp.where(lane_head == h, compact, 0.0) for h in range(width // head_size)], axis=0)
+
+    state = jnp.zeros((head_size, width), jnp.float32)
+    for block in range(outer):
+        keep = state
+        for p in range(planes):
+            if p:
+                keep = jnp.where(place == p, state, keep)
+            state = dot3(state, widen(held[p, block, :head_size])) + held[p, block, head_size:]
+        cut = slice(block * rows, (block + 1) * rows)
+        full = local_ref[cut] + dot3t(carried_ref[cut], widen(keep))
+        centred = full - exact(full, average)
+        variance = exact(centred * centred, average)
+        mixed_ref[cut] = (centred * lax.rsqrt(variance + GROUP_EPSILON) * gain_ref[...]).astype(jnp.bfloat16)
+
+    for step in range(planes - 1):
+        pair_copy(step, place).wait_send()
+    for number in range(len(lines)):
+        stat_copy(number, number).wait_send()
+
+
+def states(pair, sums, local, carried, gain, head_size, axis, pair_axis):
+    radices = radices_of(axis)
+    planes, cores = radices[1] * radices[2], lax.axis_size(pair_axis)
+    lines = radices[0] * cores - 1
+    vmem = pl.BlockSpec(memory_space=pltpu.VMEM)
+    return pl.pallas_call(
+        functools.partial(states_kernel, axis, pair_axis, radices, head_size),
+        in_specs=[vmem] * 5,
+        out_specs=[vmem] * 2,
+        out_shape=[jax.ShapeDtypeStruct(local.shape, jnp.bfloat16), jax.ShapeDtypeStruct(sums.shape, jnp.float32)],
+        scratch_shapes=[
+            pltpu.VMEM((planes,) + pair.shape, jnp.float32),
+            pltpu.VMEM((lines,) + sums.shape, jnp.float32),
+            pltpu.SemaphoreType.DMA((1,)),
+            pltpu.SemaphoreType.DMA((planes - 1,)),
+            pltpu.SemaphoreType.DMA((planes - 1,)),
+            pltpu.SemaphoreType.DMA((lines,)),
+            pltpu.SemaphoreType.DMA((lines,)),
+        ],
+        compiler_params=pltpu.CompilerParams(collective_id=1, has_side_effects=True),
+        cost_estimate=pl.CostEstimate(flops=10**9, bytes_accessed=pair.size * 16, transcendentals=0),
+        name="carry_states",
+    )(pair, sums, local, carried, gain)
+
+
+def reduce_kernel(
+    axis, pair_axis, radices,
+    state_ref, conv_ref, matrix_ref, out_ref,
+    keep, twin_out, twin_in, chain_out, chain_in,
+    twin_send, twin_recv, chain_send, chain_recv, last_send, last_recv,
+):
+    outer, middle, inner = radices
+    z, y, x = place_of(axis, radices)
+    core = lax.axis_index(pair_axis)
+    rows, half = keep.shape[1:]
+    split_at = state_ref.shape[1]
+    ways = (1, -1)
+
+    def index(z_at):
+        return (z_at * middle + y) * inner + x
+
+    def inside(at):
+        return (at >= 0) & (at < outer)
+
+    greet([{axis: index((z + step) % outer)} for step in range(1, outer)] + [{pair_axis: 1 - core}])
+
+    def twin_copy(block):
+        return pltpu.make_async_remote_copy(
+            src_ref=twin_out.at[block], dst_ref=twin_in.at[block],
+            send_sem=twin_send.at[block], recv_sem=twin_recv.at[block],
+            device_id={pair_axis: 1 - core}, device_id_type=MESH,
+        )
+
+    def chain_copy(way, steps):
+        return pltpu.make_async_remote_copy(
+            src_ref=chain_out.at[way, steps - 1], dst_ref=chain_in.at[way, steps - 1],
+            send_sem=chain_send.at[way, steps - 1], recv_sem=chain_recv.at[way, steps - 1],
+            device_id={axis: index((z + ways[way] + outer) % outer)}, device_id_type=MESH,
+        )
+
+    def product(block, side):
+        cut = pl.ds(pl.multiple_of(block * rows, rows), rows)
+        these = pl.ds(pl.multiple_of(side * half, half), half)
+        dims = (((1,), (1,)), ((), ()))
+        return lax.dot_general(
+            state_ref[cut, :], matrix_ref[these, :split_at], dims, preferred_element_type=jnp.float32
+        ) + lax.dot_general(
+            conv_ref[cut, :], matrix_ref[these, split_at:], dims, preferred_element_type=jnp.float32
+        )
+
+    def one_block(number, carry):
+        block = jnp.where(z < outer // 2, outer - 1 - number, number)
+        twin_out[block] = product(block, 1 - core).astype(jnp.bfloat16)
+        twin_copy(block).start()
+        keep[block] = product(block, core)
+        return carry
+
+    lax.fori_loop(0, outer, one_block, 0)
+
+    for steps in range(outer - 1, 0, -1):
+        for way in range(2):
+            block = z + ways[way] * steps
+
+            @pl.when(inside(block))
+            def _():
+                twin_copy(block).wait_recv()
+                keep[block] += twin_in[block].astype(jnp.float32)
+                if steps + 1 < outer:
+                    @pl.when(inside(z - ways[way]))
+                    def _():
+                        chain_copy(way, steps + 1).wait_recv()
+                        keep[block] += chain_in[way, steps].astype(jnp.float32)
+                chain_out[way, steps - 1] = keep[block].astype(jnp.bfloat16)
+                chain_copy(way, steps).start()
+
+    twin_copy(z).wait_recv()
+    keep[z] += twin_in[z].astype(jnp.float32)
+    for way in range(2):
+        @pl.when(inside(z - ways[way]))
+        def _():
+            chain_copy(way, 1).wait_recv()
+            keep[z] += chain_in[way, 0].astype(jnp.float32)
+
+    ours = pl.ds(pl.multiple_of(core * half, half), half)
+    out_ref[:, ours] = keep[z].astype(jnp.bfloat16)
+
+    def last_copy(side):
+        place = out_ref.at[:, pl.ds(pl.multiple_of(side * half, half), half)]
+        return pltpu.make_async_remote_copy(
+            src_ref=place, dst_ref=place, send_sem=last_send.at[0], recv_sem=last_recv.at[0],
+            device_id={pair_axis: 1 - core}, device_id_type=MESH,
+        )
+
+    last_copy(core).start()
+    for block in range(outer):
+        twin_copy(block).wait_send()
+    for steps in range(outer - 1, 0, -1):
+        for way in range(2):
+            @pl.when(inside(z + ways[way] * steps))
+            def _():
+                chain_copy(way, steps).wait_send()
+    last_copy(1 - core).wait_recv()
+    last_copy(core).wait_send()
+
+
+def reduce_rows(state_mixed, conv_mixed, matrix, outer, axis, pair_axis):
+    radices = radices_of(axis)
+    rows, half = state_mixed.shape[0] // outer, matrix.shape[0] // 2
+    vmem = pl.BlockSpec(memory_space=pltpu.VMEM)
+    slots = (2, outer - 1)
+    return pl.pallas_call(
+        functools.partial(reduce_kernel, axis, pair_axis, radices),
+        in_specs=[vmem] * 3,
+        out_specs=vmem,
+        out_shape=jax.ShapeDtypeStruct((rows, 2 * half), jnp.bfloat16),
+        scratch_shapes=[
+            pltpu.VMEM((outer, rows, half), jnp.float32),
+            pltpu.VMEM((outer, rows, half), jnp.bfloat16),
+            pltpu.VMEM((outer, rows, half), jnp.bfloat16),
+            pltpu.VMEM(slots + (rows, half), jnp.bfloat16),
+            pltpu.VMEM(slots + (rows, half), jnp.bfloat16),
+            pltpu.SemaphoreType.DMA((outer,)),
+            pltpu.SemaphoreType.DMA((outer,)),
+            pltpu.SemaphoreType.DMA(slots),
+            pltpu.SemaphoreType.DMA(slots),
+            pltpu.SemaphoreType.DMA((1,)),
+            pltpu.SemaphoreType.DMA((1,)),
+        ],
+        compiler_params=pltpu.CompilerParams(collective_id=2, has_side_effects=True, vmem_limit_bytes=60 * 2**20),
+        cost_estimate=pl.CostEstimate(flops=10**9, bytes_accessed=matrix.size * 8, transcendentals=0),
+        name="reduce_rows",
+    )(state_mixed, conv_mixed, matrix)
+
+
+def delta_blocks_kernel(head_size, chunk, block, *refs):
+    ins, (local_ref, carried_ref, pair_ref), scratch = refs[:7], refs[7:10], refs[10]
+    delta_kernel(head_size, chunk, block, *ins, local_ref, carried_ref, scratch)
+    width = scratch.shape[-1]
+    for first in range(2):
+        total = jnp.zeros((head_size, width), jnp.float32)
+        for h in range(width // head_size):
+            at = first * width + h * head_size
+            total = total + scratch[0, at : at + head_size]
+        pair_ref[0, first * head_size : (first + 1) * head_size] = total
+
+
+def delta_blocks(query, key, value, decay_pre, rate_pre, factor, share, blocks, head_size):
+    total, width = query.shape
+    rows, heads = total // blocks, factor.shape[1]
+    block = math.gcd(rows, 128)
+    chunk = math.gcd(block, 16)
+    wide = pl.BlockSpec((rows, width), lambda i: (i, 0))
+    thin = pl.BlockSpec((rows, heads), lambda i: (i, 0))
+    return pl.pallas_call(
+        functools.partial(delta_blocks_kernel, head_size, chunk, block),
+        grid=(blocks,),
+        in_specs=[wide] * 5 + [thin] * 2,
+        out_specs=[wide, wide, pl.BlockSpec((1, 2 * head_size, width), lambda i: (i, 0, 0))],
+        out_shape=[
+            jax.ShapeDtypeStruct((total, width), jnp.float32),
+            jax.ShapeDtypeStruct((total, width), jnp.float32),
+            jax.ShapeDtypeStruct((blocks, 2 * head_size, width), jnp.float32),
+        ],
+        scratch_shapes=[pltpu.VMEM((1, 2 * width, width), jnp.float32)],
+        cost_estimate=pl.CostEstimate(
+            flops=total * width * width * 60, bytes_accessed=total * width * 32, transcendentals=total * width * 10
+        ),
+        name="delta_chunks",
+    )(query, key, value, decay_pre, rate_pre, factor, share)
+
+
+def body(*args):
+    outer, middle, inner = radices_of("sp")
+    heads, channels = args[13].shape[1], args[2].shape[1]
+    width = channels // outer
+    fits = (
+        lax.axis_size("tp") == 2 and outer > 1 and middle == 2 and inner == 2
+        and heads % outer == 0 and width == 128 and args[5].shape[1] % (128 * outer) == 0
+    )
+    return fast_body(*args) if fits else plain_body(*args)
+
+
+def fast_body(
+    tokens,
+    input_norm_gain,
+    query_matrix,
+    key_matrix,
+    value_matrix,
+    convolution_value_matrix,
+    convolution_gate_matrix,
+    decay_offset_channel,
+    decay_first_matrix,
+    decay_second_matrix,
+    learning_rate_offset,
+    learning_rate_first_matrix,
+    learning_rate_second_matrix,
+    forgetting_rate_factor,
+    state_retention_share,
+    per_head_norm_gain,
+    convolution_filter_taps,
+    convolution_channel_gain,
+    attention_output_matrix,
+    convolution_output_matrix,
+):
+    outer, middle, inner = radices_of("sp")
+    planes = middle * inner
+    rows = tokens.shape[0]
+    heads, channels = forgetting_rate_factor.shape[1], query_matrix.shape[1]
+    head_size = channels // heads
+    z = lax.axis_index("sp") // planes
+
+    def quarter(value, axis=-1):
+        size = value.shape[axis] // outer
+        return lax.dynamic_slice_in_dim(value, z * size, size, axis)
+
+    widened = tokens.astype(jnp.float32)
+    normed = (
+        widened
+        * lax.rsqrt(jnp.mean(widened * widened, axis=-1, keepdims=True) + RMS_EPSILON)
+        * input_norm_gain
+    ).astype(jnp.bfloat16)
+    side = jnp.concatenate([forgetting_rate_factor.T, state_retention_share.T], axis=0)
+    weights = (
+        query_matrix, key_matrix, value_matrix, convolution_value_matrix, convolution_gate_matrix,
+        attention_output_matrix, convolution_output_matrix,
+    )
+    normed, side, (heads_in, conv_in, both_out) = spread(normed, side, weights, ((0, 1, 2), (3, 4), (5, 6)), "sp", "tp")
+    normed = normed.reshape(-1, normed.shape[-1])
+
+    width = channels // outer
+    projected = [
+        jnp.dot(normed, heads_in[:, i * width : (i + 1) * width], preferred_element_type=jnp.float32) for i in range(3)
+    ]
+    conv_width = conv_in.shape[1] // 2
+    conv_value = jnp.dot(normed, conv_in[:, :conv_width], preferred_element_type=jnp.float32)
+    conv_gate = jnp.dot(normed, conv_in[:, conv_width:], preferred_element_type=jnp.float32)
+    decay_mid = jnp.tanh(jnp.dot(normed, decay_first_matrix, preferred_element_type=jnp.float32)).astype(jnp.bfloat16)
+    rate_mid = jnp.dot(normed, learning_rate_first_matrix, preferred_element_type=jnp.float32).astype(jnp.bfloat16)
+    decay_pre = quarter(decay_offset_channel) + jnp.dot(
+        decay_mid, quarter(decay_second_matrix), preferred_element_type=jnp.float32
+    )
+    rate_pre = quarter(learning_rate_offset) + jnp.dot(
+        rate_mid, quarter(learning_rate_second_matrix), preferred_element_type=jnp.float32
+    )
+    few = quarter(side.reshape(outer, 2, heads, rows), 2).transpose(1, 0, 3, 2).reshape(2, outer * rows, heads // outer)
+
+    gated = (conv_value * jax.nn.sigmoid(conv_gate)).astype(jnp.bfloat16).reshape(outer, rows, conv_width)
+    span = convolution_filter_taps.shape[0]
+    ring = [
+        (at * planes + p, at * planes + (p + 1) % planes) for at in range(outer) for p in range(planes)
+    ]
+    rim = lax.ppermute(gated[:, rows - (span - 1) :], "sp", ring)
+    shifted = jnp.concatenate([jnp.zeros_like(rim[:1]), rim[:-1]], axis=0)
+    rim = jnp.where(lax.axis_index("sp") % planes == 0, shifted, rim)
+    padded = jnp.concatenate([rim, gated], axis=1)
+    taps = quarter(convolution_filter_taps)
+    filtered = jnp.zeros(gated.shape, jnp.float32)
+    for offset in range(span):
+        filtered = filtered + taps[offset] * padded[:, offset : offset + rows]
+    filtered = filtered.reshape(outer * rows, conv_width)
+    sums = jnp.stack([jnp.sum(filtered, axis=-1), jnp.sum(filtered * filtered, axis=-1)])
+
+    local, carried, pair = delta_blocks(*projected, decay_pre, rate_pre, few[0], few[1], outer, head_size)
+    state_mixed, totals = states(
+        pair, sums, local, carried, quarter(per_head_norm_gain)[None], head_size, "sp", "tp"
+    )
+    conv_channels = conv_width * outer * lax.axis_size("tp")
+    row_mean = totals[0] / conv_channels
+    deviation = filtered - row_mean[:, None]
+    variance = totals[1] / conv_channels - row_mean * row_mean
+    conv_mixed = jax.nn.silu(
+        deviation * lax.rsqrt(variance + LAYER_EPSILON)[:, None] * quarter(convolution_channel_gain)
+    ).astype(jnp.bfloat16)
+    return reduce_rows(state_mixed, conv_mixed, both_out, outer, "sp", "tp")
+
+
 def solution(mesh):
     return jax.shard_map(
         body,

time: 364 us -> 261 us (0.72)
  starting transfers between devices: 85.5 us -> 0.35 us
  waiting for transfers between devices: 36.3 us -> 0.01 us
  Pallas kernels: 185 us -> 212 us
  between operations: 13.5 us -> 0.17 us
  local copies, waits for them, and re-layouts: 5.86 us -> 11.1 us
  other arithmetic: 8.63 us -> 13 us
    ppermute x7 -> x1, starting transfers between devices: 85.3 us -> 0.35 us  [fast_body(): rim = lax.ppermute(gated[:, rows - (span - 1):], 'sp', ring)]
    pallas_call x3 -> x4, Pallas kernels: 185 us -> 212 us  [the longest x1 88.7 us: spread(): pl.pallas_call(functools.partial(spread_kernel, axis, pair_axis, radices,...]
    ppermute x7 -> x1, waiting for transfers between devices: 25.3 us -> 0.01 us  [fast_body(): rim = lax.ppermute(gated[:, rows - (span - 1):], 'sp', ring)]
    all_gather x4 -> x0, waiting for transfers between devices: 8.87 us -> none  [the longest x2 8.85 us: body(): lax.all_gather((attention_output_matrix, convolution_output_matrix), 'sp'...]
    dot_general x13 -> x7, matrix products: 25.7 us -> 22.6 us  [the longest x3 8.52 us: fast_body(): jnp.dot(normed, heads_in[:, i * width:(i + 1) * width], preferred_element...]
  transfers between devices with their start and end apart: 11 -> 1, of which waited for: 7 -> 0; matrix products, arithmetic and copies ran while one was open for 10% -> 10% of each run, Pallas kernels for 51% -> 22%
where the time goes in v1:
time: 261 us; the launch traced here: 260 us
  Pallas kernels  212 us (81%)
  matrix products  22.6 us (9%)
  other arithmetic  13 us (5%)
  local copies, waits for them, and re-layouts  11.1 us (4%)
    pallas_call x1, Pallas kernels, spread(): pl.pallas_call(functools.partial(spread_kernel, axis, pair_axis, radices,...  88.7 us
    pallas_call x1, Pallas kernels, delta_blocks(): pl.pallas_call(functools.partial(delta_blocks_kernel, head_size, chunk, b...  56.7 us
    pallas_call x1, Pallas kernels, reduce_rows(): pl.pallas_call(functools.partial(reduce_kernel, axis, pair_axis, radices)...  45.6 us
    pallas_call x1, Pallas kernels, states(): pl.pallas_call(functools.partial(states_kernel, axis, pair_axis, radices,...  21.5 us
    dot_general x3, matrix products, fast_body(): jnp.dot(normed, heads_in[:, i * width:(i + 1) * width], preferred_element...  8.52 us
  transfers between devices with their start and end apart: 1, of which 0 were waited for; matrix products, arithmetic and copies ran while one was open for 10% of the time, Pallas kernels for 22%

profile of v1, /device:TPU:0, one launch (start us, length us, event | category | flops | bytes accessed | tf_op | source)
XLA Modules:
  0.0 259.7 jit_solution(2066400953357027)
XLA Ops:
  0.0 1.6 fusion
  1.6 2.5 fusion.2.refs_0_
  4.1 1.3 pad_maximum_fusion.1.refs_1_
  5.4 88.7 %spread_weights.1 = (bf16[4,256,2048]{2,1,0:T(8,128)(2,1)}, f32[4,16,256]{2,1,0:T(8,128)}, bf16[4,2,2,128,384]{4,3,2,1,0:T(8,128)(2,1)}, bf16[4,2,2,128,512]{4,3...) custom-call(bf16[256,2048]{1,0:T(8,128)(2,1)} %fusion.2.refs_0_, f32[16,256]{1,0:T(8,128)} %pad_maximum_fusion.1.refs_1_, ...), custom_call_target="tpu_custom_call" | custom-call | flops 1000000000 | bytes 8388608 | tf_op jit(solution)/shard_map/spread_weights/pallas_call | solution.py:608
  94.2 3.9 %fusion.5 = f32[1024,256]{1,0:T(8,128)S(1)} fusion(bf16[1024,2048]{1,0:T(8,128)(2,1)} %bitcast.115, bf16[2048,512]{1,0:T(8,128)(2,1)} %bitcast.122), kind=kOutput, calls=%fused_computation.38 | convolution fusion | flops 1074528256 | bytes 6291456 | tf_op jit(solution)/shard_map/dot_general | solution.py:973
  98.6 1.3 fusion.6
  100.2 4.4 %fusion.41.refs_2_ = f32[1024,128]{1,0:T(8,128)} fusion(bf16[1024,2048]{1,0:T(8,128)(2,1)} %bitcast.116, bf16[2048,384]{1,0:T(8,128)(2,1)S(1)} %bitcast.125), kind=kOutput, calls=%fused_computation.91 | convolution fusion | flops 536870912 | bytes 5242880 | tf_op jit(solution)/shard_map/dot_general | solution.py:969
  104.7 2.1 fusion.43.refs_1_
  106.7 2.0 fusion.45.refs_0_
  108.8 0.8 constant_dynamic-slice_fusion.1
  110.0 1.2 fusion.52
  112.6 1.3 dynamic-slice_bitcast_fusion.gain_ref
  113.9 0.8 dynamic_slice.31
  114.7 4.4 %convolution_add_fusion.refs_4_ = f32[1024,128]{1,0:T(8,128)} fusion(bf16[1024,2048]{1,0:T(8,128)(2,1)} %bitcast.117, bf16[2048,128]{1,0:T(8,128)(2,1)S(1)} %copy-done, f32[128]{0:T(128)S(1)} %dynamic_slice.26, bf16[128,512]{1,0:T(8,128)(2,1)} %param.32, s32[]{:T(128)S(6)} %select_n.34), kind=kOutput, calls=%fused_computation.40 | convolution fusion | flops 570687488 | bytes 5276164 | tf_op jit(solution)/shard_map/dot_general | solution.py:979
  119.1 4.5 %convolution_add_fusion.1.refs_3_ = f32[1024,128]{1,0:T(8,128)} fusion(bf16[1024,2048]{1,0:T(8,128)(2,1)} %bitcast.118, bf16[2048,128]{1,0:T(8,128)(2,1)S(1)} %copy-done.1, f32[128]{0:T(128)S(1)} %dynamic_slice.24, bf16[128,512]{1,0:T(8,128)(2,1)} %param.29, s32[]{:T(128)S(6)} %select_n.34), kind=kOutput, calls=%fused_computation.41 | convolution fusion | flops 570687488 | bytes 5276164 | tf_op jit(solution)/shard_map/dot_general | solution.py:976
  123.6 1.2 fusion.53
  124.8 1.2 constant_dynamic-slice_fusion
  126.0 56.7 %delta_chunks.1 = (f32[1024,128]{1,0:T(8,128)}, f32[1024,128]{1,0:T(8,128)}, f32[4,128,128]{2,1,0:T(8,128)}) custom-call(f32[1024,128]{1,0:T(8,128)} %fusion.45.refs_0_, f32[1024,128]{1,0:T(8,128)} %fusion.43.refs_1_, f32[1024,128]{1,0:T(8,128)} %fusion.41.refs_2_, f32[1024,128]{1,0:T(8,128)} %convolution_add_fusion.1.refs_3_, ...), custom_call_target="tpu_custom_call" | custom-call | flops 1006632960 | bytes 4194304 | tf_op jit(solution)/shard_map/delta_chunks/pallas_call | solution.py:891
  182.6 5.0 %fusion.51 = (f32[4,256]{1,0:T(4,128)S(1)}, f32[4,256]{1,0:T(4,128)S(1)}, f32[4,256,256]{2,1,0:T(8,128)S(1)}) fusion(bf16[4,256,256]{2,1,0:T(8,128)(2,1)S(1)} %bitcast.71, f32[256]{0:T(256)S(1)} %bitcast.96, bf16[4,30,256]{2,1,0:T(8,128)(2,1)S(1)} %pad_select_fusion, f32[256]{0:T(256)S(1)} %bitcast.98, f32[256]{0:T(256)S(1)} %bitcast.99, ...), kind=kLoop, calls=%fused_computation.111 | loop fusion | flops 48494592 | bytes 1674240 | tf_op jit(solution)/shard_map/reduce_sum | solution.py:998
  188.3 21.5 %carry_states.1 = (bf16[1024,128]{1,0:T(8,128)(2,1)}, f32[2,1024]{1,0:T(2,128)}) custom-call(f32[4,128,128]{2,1,0:T(8,128)} %get-tuple-element.18.pair_ref, f32[2,1024]{1,0:T(2,128)} %pad_maximum_fusion.2.sums_ref, f32[1024,128]{1,0:T(8,128)} %get-tuple-element.20.local_ref, f32[1024,128]{1,0:T(8,128)} %get-tuple-element.21.carried_ref, ...), custom_call_target="tpu_custom_call" | custom-call | flops 1000000000 | bytes 1048576 | tf_op jit(solution)/shard_map/carry_states/pallas_call | solution.py:723
  209.8 0.8 slice_multiply_fusion.1
  210.6 1.2 multiply_convert_fusion.conv_ref
  211.8 45.6 %reduce_rows.1 = bf16[256,2048]{1,0:T(8,128)(2,1)} custom-call(bf16[1024,128]{1,0:T(8,128)(2,1)} %get-tuple-element.22.state_ref, bf16[1024,256]{1,0:T(8,128)(2,1)} %multiply_convert_fusion.conv_ref, bf16[2048,384]{1,0:T(8,128)(2,1)} %bitcast.124), custom_call_target="tpu_custom_call" | custom-call | flops 1000000000 | bytes 6291456 | tf_op jit(solution)/shard_map/reduce_rows/pallas_call | solution.py:848
  257.4 2.3 copy.26
  (25 shorter events, 3.4 us)
Async XLA Ops:
  0.0 114.7 %copy-start = (bf16[2048,128]{1,0:T(8,128)(2,1)S(1)}, bf16[2048,128]{1,0:T(8,128)(2,1)}, u32[]{:S(2)}) copy-start(bf16[2048,128]{1,0:T(8,128)(2,1)} %param.31) | copy-start | bytes 1572868
  94.1 3.9 %copy-start.2 = (bf16[4,256,2048]{2,1,0:T(8,128)(2,1)S(1)}, bf16[4,256,2048]{2,1,0:T(8,128)(2,1)}, u32[]{:S(2)}) copy-start(bf16[4,256,2048]{2,1,0:T(8,128)(2,1)} %get-tuple-element.15) | copy-start | bytes 12582916
  94.2 4.4 %copy-start.4 = (bf16[4,2,2,128,512]{4,3,2,1,0:T(8,128)(2,1)S(1)}, bf16[4,2,2,128,512]{4,3,2,1,0:T(8,128)(2,1)}, u32[]{:S(2)}) copy-start(bf16[4,2,2,128,512]{4,3,2,1,0:T(8,128)(2,1)} %get-tuple-element.19) | copy-start | bytes 6291460
  98.6 1.6 copy-start.5
  99.9 82.7 %collective-permute-start = (bf16[4,30,256]{2,1,0:T(8,128)(2,1)S(1)}, bf16[4,30,256]{2,1,0:T(8,128)(2,1)S(1)}, u32[]{:S(2)}, u32[]{:S(2)}) collective-permute-start(bf16[4,30,256]{2,1,0:T(8,128)(2,1)S(1)} %slice.297), channel_id=1, source_target_pairs={{0,2},{2,4},{4,6},{6,0},{8,10},{10,12},{12,14},{14,8},{16,18},{18,... | collective-permute-start | bytes 184328 | tf_op jit(solution)/shard_map/ppermute | solution.py:989
  100.2 4.4 %copy-start.3 = (bf16[4,256,2048]{2,1,0:T(8,128)(2,1)S(1)}, bf16[4,256,2048]{2,1,0:T(8,128)(2,1)}, u32[]{:S(2)}) copy-start(bf16[4,256,2048]{2,1,0:T(8,128)(2,1)} %get-tuple-element.15) | copy-start | bytes 12582916
  109.6 9.5 %copy-start.1 = (bf16[2048,128]{1,0:T(8,128)(2,1)S(1)}, bf16[2048,128]{1,0:T(8,128)(2,1)}, u32[]{:S(2)}) copy-start(bf16[2048,128]{1,0:T(8,128)(2,1)} %param.28) | copy-start | bytes 1572868

commit v2 on v1

--- a/solution.py
+++ b/solution.py
@@ -430,16 +430,25 @@
     pl.semaphore_wait(barrier, len(devices))
 
 
-def spread_kernel(axis, pair_axis, radices, widths, placed, *refs):
+def spread_kernel(axis, pair_axis, radices, widths, placed, firsts, early, head_size, chunk, block, *refs):
     number = len(widths)
-    tokens_ref, side_ref, ins = refs[0], refs[1], refs[2 : 2 + number]
+    raw_ref, gain_ref, side_ref, ins = refs[0], refs[1], refs[2], refs[3 : 3 + number]
+    refs = refs[3 + number :]
+    extra, (decay_ref, rate_ref, decay_offset_ref, rate_offset_ref) = refs[: len(firsts)], refs[len(firsts) : len(firsts) + 4]
+    refs = refs[len(firsts) + 4 :]
     kinds = 1 + max(out for out, _ in placed)
-    tokens_out, side_out, outs = refs[2 + number], refs[3 + number], refs[4 + number : 4 + number + kinds]
-    (own_sem, far_send, far_recv, near_send, near_recv, side_send, side_recv,
-     tok_send, tok_recv, sib_send, sib_recv) = refs[4 + number + kinds :]
+    tokens_all, local_ref, carried_ref, pair_ref = refs[:4]
+    later, refs = refs[4 : 3 + kinds], refs[3 + kinds :]
+    (first_out, tokens_out, side_out, tokens_ref, proj, mats, adds, hist, queries,
+     first_sem, own_sem, far_send, far_recv, near_send, near_recv, side_send, side_recv,
+     tok_send, tok_recv, sib_send, sib_recv) = refs
+    outs = [first_out, *later]
     outer, middle, inner = radices
     z, y, x = place_of(axis, radices)
     core = lax.axis_index(pair_axis)
+    widened = raw_ref[...].astype(jnp.float32)
+    scale = lax.rsqrt(jnp.mean(widened * widened, axis=-1, keepdims=True) + RMS_EPSILON)
+    tokens_ref[...] = (widened * scale * gain_ref[...]).astype(jnp.bfloat16)
     half = tokens_ref.shape[0] // 2
     mine, other = pl.ds(pl.multiple_of(core * half, half), half), pl.ds(pl.multiple_of((1 - core) * half, half), half)
 
@@ -457,9 +466,9 @@
     def part(w, at):
         return ins[w].at[:, pl.ds(pl.multiple_of(at * widths[w], widths[w]), widths[w])]
 
-    def slot(w, *where):
+    def slot(w, *where, cut=slice(None)):
         out, offset = placed[w]
-        return outs[out].at[(*where, slice(None), pl.ds(offset, widths[w]))]
+        return outs[out].at[(*where, cut, pl.ds(offset, widths[w]))]
 
     def far_copy(w, step, to, z_from):
         return pltpu.make_async_remote_copy(
@@ -475,22 +484,28 @@
             device_id={axis: index(to, y, x)}, device_id_type=MESH,
         )
 
-    def near_copy(w, order, stage, y_at, x_at):
+    names = list(near)
+    depth = ins[0].shape[0]
+    orders = [names, names[::-1]]
+
+    def near_copy(w, part_at, stage, y_at, x_at):
+        order = orders[part_at]
+        cut = pl.ds(part_at * (depth // 2), depth // 2)
         if stage == 0:
-            region = slot(w, slice(None), y_at, x_at)
+            region = slot(w, slice(None), y_at, x_at, cut=cut)
         elif order[0] == "x":
-            region = slot(w, slice(None), y_at, slice(None))
+            region = slot(w, slice(None), y_at, slice(None), cut=cut)
         else:
-            region = slot(w, slice(None), slice(None), x_at)
+            region = slot(w, slice(None), slice(None), x_at, cut=cut)
         return pltpu.make_async_remote_copy(
             src_ref=region, dst_ref=region,
-            send_sem=near_send.at[w, stage], recv_sem=near_recv.at[w, stage],
+            send_sem=near_send.at[w, part_at, stage], recv_sem=near_recv.at[w, part_at, stage],
             device_id={axis: near[order[stage]]}, device_id_type=MESH,
         )
 
-    def theirs(w, order, stage):
-        y_at, x_at = (y, 1 - x) if order[stage] == "x" else (1 - y, x)
-        return near_copy(w, order, stage, y_at, x_at)
+    def theirs(w, part_at, stage):
+        y_at, x_at = (y, 1 - x) if orders[part_at][stage] == "x" else (1 - y, x)
+        return near_copy(w, part_at, stage, y_at, x_at)
 
     def inside(at):
         return (at >= 0) & (at < outer)
@@ -522,29 +537,40 @@
     own.append(pltpu.make_async_copy(side_ref, side_out.at[z], own_sem.at[number + 1]))
     for step in range(outer - 1):
         side_copy(step, far[step], z).start()
-    for w in range(number):
-        own[w].start()
-        for step in range(outer - 1):
-            far_copy(w, step, far[step], z).start()
+    def send_far(some):
+        for w in some:
+            own[w].start()
+            for step in range(outer - 1):
+                far_copy(w, step, far[step], z).start()
+
+    send_far(early)
     for way in range(2):
         @pl.when(sends(way, 0))
         def _():
             token_copy(way, 0, z, tokens_ref.at[mine]).start()
     own[number].start()
     own[number + 1].start()
-
-    names = list(near)
-    orders = [names if w % 2 == 0 else names[::-1] for w in range(number)]
+    kept = []
+    for item, (out, offset) in enumerate(firsts):
+        for at in range(outer * middle * inner):
+            where = (at // (middle * inner), (at // inner) % middle, at % inner)
+            kept.append(pltpu.make_async_copy(
+                extra[item].at[at * depth : (at + 1) * depth],
+                outs[out].at[(*where, slice(None), pl.ds(offset, extra[item].shape[1]))],
+                first_sem.at[item, at],
+            ))
+            kept[-1].start()
 
     def advance(w, stage):
         if stage == 0:
             own[w].wait()
             for step in range(outer - 1):
                 far_copy(w, step, far[step], (z + outer - step - 1) % outer).wait_recv()
-        else:
-            theirs(w, orders[w], stage - 1).wait_recv()
-        if stage < len(names):
-            near_copy(w, orders[w], stage, y, x).start()
+        for part_at in range(2):
+            if stage:
+                theirs(w, part_at, stage - 1).wait_recv()
+            if stage < len(names):
+                near_copy(w, part_at, stage, y, x).start()
 
     def token_step(step):
         for way in range(2):
@@ -552,36 +578,106 @@
             @pl.when(inside(block))
             def _():
                 token_copy(way, step, block, tokens_out.at[block, mine]).wait_recv()
-                if step + 1 < outer - 1:
-                    @pl.when(sends(way, step + 1))
-                    def _():
-                        token_copy(way, step + 1, block, tokens_out.at[block, mine]).start()
+                @pl.when(sends(way, step + 1) & (step + 1 < outer - 1))
+                def _():
+                    token_copy(way, step + 1, block, tokens_out.at[block, mine]).start()
                 sibling_copy(way, step, block, mine).start()
 
     last = len(names)
-    steps = 0
-    for tick in range(number + last):
-        for stage in range(last, -1, -1):
-            w = tick - stage
-            if 0 <= w < number:
-                advance(w, stage)
-        if tick >= number - 1 and steps < outer - 1:
-            token_step(steps)
-            steps += 1
-    while steps < outer - 1:
-        token_step(steps)
-        steps += 1
+
+    def sibling_step(step):
+        for way in range(2):
+            block = arrived(way, step)
+            @pl.when(inside(block))
+            def _():
+                sibling_copy(way, step, block, other).wait_recv()
+
+    def run(some):
+        for tick in range(len(some) + last):
+            for stage in range(last + 1):
+                if 0 <= tick - stage < len(some):
+                    advance(some[tick - stage], stage)
+
+    run(early)
     own[number].wait()
     own[number + 1].wait()
+    for item in kept:
+        item.wait()
     for step in range(outer - 1):
         side_copy(step, far[step], (z + outer - step - 1) % outer).wait_recv()
+    token_step(0)
+    rest = [[w for w in range(number) if placed[w][0] == out] for out in range(1, kinds)]
+    one_block, chain, read = delta_phases(
+        z, head_size, chunk, block, proj, side_out, decay_ref, rate_ref, decay_offset_ref, rate_offset_ref,
+        local_ref, carried_ref, pair_ref, mats, adds, hist, queries,
+    )
+    pieces = tokens_ref.shape[0] // block
+    edge = jnp.minimum(z, outer - 1 - z)
+    toward = jnp.where(z < outer // 2, -1, 1)
+    piece_depth = middle * inner * depth
+
+    def project(group):
+        total = None
+        for part_at in range(outer):
+            matrix = first_out[part_at].reshape(piece_depth, first_out.shape[-1])
+            term = jnp.dot(
+                tokens_out[group, :, part_at * piece_depth : (part_at + 1) * piece_depth], matrix,
+                preferred_element_type=jnp.float32,
+            )
+            total = term if total is None else total + term
+        proj[...] = total
+
+    def one_round(k, carry):
+        twosided = k <= 2 * edge
+        distance = jnp.where(twosided, (k + 1) // 2, k - edge)
+        side = jnp.where(twosided & (k % 2 == 1), toward, -toward)
+        group = z + side * distance
+
+        @pl.when(k > 0)
+        def _():
+            sibling_step(k - 1)
+
+        project(group)
+        for piece in range(pieces):
+            one_block(group, piece)
+            if piece == 0:
+                @pl.when((k > 0) & (k < outer - 1))
+                def _():
+                    token_step(k)
+
+                for at, some in enumerate(rest):
+                    @pl.when(k == at)
+                    def _():
+                        send_far(some)
+
+                    for stage in range(last):
+                        @pl.when(k == at + 2 + stage)
+                        def _():
+                            for w in some:
+                                advance(w, stage)
+        return carry
+
+    lax.fori_loop(0, outer, one_round, 0)
+    keep_tokens = pltpu.make_async_copy(tokens_out, tokens_all, own_sem.at[number + 2])
+    keep_tokens.start()
+    chain()
+    for at, some in enumerate(rest):
+        for stage in range(last + 1):
+            if at + 2 + stage >= outer and stage < last:
+                for w in some:
+                    advance(w, stage)
+    read()
+    for some in rest:
+        for w in some:
+            advance(w, last)
+    keep_tokens.wait()
+    for step in range(outer - 1):
         side_copy(step, far[step], z).wait_send()
     for step in range(outer - 1):
         for way in range(2):
             block = arrived(way, step)
             @pl.when(inside(block))
             def _():
-                sibling_copy(way, step, block, other).wait_recv()
                 sibling_copy(way, step, block, mine).wait_send()
             @pl.when(sends(way, step))
             def _():
@@ -590,10 +686,11 @@
         for step in range(outer - 1):
             far_copy(w, step, far[step], z).wait_send()
         for stage in range(last):
-            near_copy(w, orders[w], stage, y, x).wait_send()
-
-
-def spread(normed, side, weights, groups, axis, pair_axis):
+            for part_at in range(2):
+                near_copy(w, part_at, stage, y, x).wait_send()
+
+
+def spread(tokens, gain, side, weights, groups, firsts, maps, head_size, axis, pair_axis):
     radices = radices_of(axis)
     outer, number = radices[0], len(weights)
     widths = [item.shape[1] // outer for item in weights]
@@ -604,22 +701,44 @@
             placed[w] = (out, offset)
             offset += widths[w]
         totals.append(offset)
-    depth = weights[0].shape[0]
+    extras, width = [], widths[0]
+    for item in firsts:
+        extras.append((0, totals[0]))
+        totals[0] += item.shape[1]
+    depth, rows = weights[0].shape[0], tokens.shape[0]
+    block = math.gcd(rows, 128)
+    chunk = math.gcd(block, 32)
+    total = outer * rows
+    vmem, hbm = pl.BlockSpec(memory_space=pltpu.VMEM), pl.BlockSpec(memory_space=pl.ANY)
     outs = pl.pallas_call(
-        functools.partial(spread_kernel, axis, pair_axis, radices, widths, placed),
-        in_specs=[pl.BlockSpec(memory_space=pltpu.VMEM)] * (2 + number),
-        out_specs=[pl.BlockSpec(memory_space=pl.ANY)] * (2 + len(groups)),
+        functools.partial(
+            spread_kernel, axis, pair_axis, radices, widths, placed, extras, groups[0], head_size, chunk, block
+        ),
+        in_specs=[vmem] * (3 + number + len(firsts) + len(maps)),
+        out_specs=[hbm] + [vmem] * 3 + [hbm] * (len(groups) - 1),
         out_shape=[
-            jax.ShapeDtypeStruct((outer,) + normed.shape, normed.dtype),
-            jax.ShapeDtypeStruct((outer,) + side.shape, side.dtype),
+            jax.ShapeDtypeStruct((outer,) + tokens.shape, tokens.dtype),
+            jax.ShapeDtypeStruct((total, width), jnp.float32),
+            jax.ShapeDtypeStruct((total, width), jnp.float32),
+            jax.ShapeDtypeStruct((outer, width, width), jnp.float32),
         ]
-        + [jax.ShapeDtypeStruct(radices + (depth, total), weights[0].dtype) for total in totals],
+        + [jax.ShapeDtypeStruct(radices + (depth, size), weights[0].dtype) for size in totals[1:]],
         scratch_shapes=[
-            pltpu.SemaphoreType.DMA((number + 2,)),
+            pltpu.VMEM(radices + (depth, totals[0]), weights[0].dtype),
+            pltpu.VMEM((outer,) + tokens.shape, tokens.dtype),
+            pltpu.VMEM((outer,) + side.shape, side.dtype),
+            pltpu.VMEM(tokens.shape, tokens.dtype),
+            pltpu.VMEM((rows, totals[0]), jnp.float32),
+        ]
+        + [pltpu.VMEM((total // chunk, width, width), jnp.float32)] * 3
+        + [
+            pltpu.VMEM((total, width), jnp.float32),
+            pltpu.SemaphoreType.DMA((len(firsts), math.prod(radices))),
+            pltpu.SemaphoreType.DMA((number + 3,)),
             pltpu.SemaphoreType.DMA((number, outer - 1)),
             pltpu.SemaphoreType.DMA((number, outer - 1)),
-            pltpu.SemaphoreType.DMA((number, 2)),
-            pltpu.SemaphoreType.DMA((number, 2)),
+            pltpu.SemaphoreType.DMA((number, 2, 2)),
+            pltpu.SemaphoreType.DMA((number, 2, 2)),
             pltpu.SemaphoreType.DMA((outer - 1,)),
             pltpu.SemaphoreType.DMA((outer - 1,)),
             pltpu.SemaphoreType.DMA((2, outer - 1)),
@@ -627,11 +746,18 @@
             pltpu.SemaphoreType.DMA((2, outer - 1)),
             pltpu.SemaphoreType.DMA((2, outer - 1)),
         ],
-        compiler_params=pltpu.CompilerParams(collective_id=0, has_side_effects=True),
-        cost_estimate=pl.CostEstimate(flops=10**9, bytes_accessed=2 * normed.size * 2 * outer, transcendentals=0),
-        name="spread_weights",
-    )(normed, side, *weights)
-    return outs[0], outs[1], [out.reshape(-1, total) for out, total in zip(outs[2:], totals)]
+        compiler_params=pltpu.CompilerParams(collective_id=0, has_side_effects=True, vmem_limit_bytes=60 * 2**20),
+        cost_estimate=pl.CostEstimate(flops=10**10, bytes_accessed=8 * tokens.size * outer, transcendentals=0),
+        name="spread_and_delta",
+    )(tokens, gain, side, *weights, *firsts, *maps)
+    return outs[:4], [out.reshape(-1, size) for out, size in zip(outs[4:], totals[1:])]
+
+
+def spread_sum(values, matrix):
+    top, rest = split(values)
+    return jnp.dot(top, matrix, preferred_element_type=jnp.float32) + jnp.dot(
+        rest, matrix, preferred_element_type=jnp.float32
+    )
 
 
 def states_kernel(
@@ -688,25 +814,39 @@
     for step in range(planes - 1):
         pair_copy(step, (place + planes - step - 1) % planes).wait_recv()
 
-    lane_head = lax.broadcasted_iota(jnp.int32, (1, width), 1) // head_size
-    row_w = lax.broadcasted_iota(jnp.int32, (width, width), 0)
-    col_w = lax.broadcasted_iota(jnp.int32, (width, width), 1)
-    average = jnp.where((row_w // head_size) == (col_w // head_size), 1.0 / head_size, 0.0)
-
-    def widen(compact):
-        return jnp.concatenate([jnp.where(lane_head == h, compact, 0.0) for h in range(width // head_size)], axis=0)
-
-    state = jnp.zeros((head_size, width), jnp.float32)
+    row = lax.broadcasted_iota(jnp.int32, (width, width), 0)
+    lane = lax.broadcasted_iota(jnp.int32, (width, width), 1)
+    average = jnp.where((row // head_size) == (lane // head_size), 1.0 / head_size, 0.0).astype(jnp.bfloat16)
+    first_head, moves = row < head_size, lane < head_size
+
+    def step_matrix(item):
+        part = jnp.where(moves, item, 0.0)
+        return jnp.where(first_head, part, pltpu.roll(part, head_size, 1))
+
+    def state_matrix(item):
+        part = jnp.where(moves, 0.0, item)
+        return jnp.where(first_head, pltpu.roll(part, head_size, 1), part)
+
+    def compose(earlier, later):
+        return dot3(step_matrix(later), earlier) + jnp.where(moves, 0.0, later)
+
+    nothing = jnp.where(moves & (row % head_size == lane), 1.0, 0.0)
+    before, whole = [], []
     for block in range(outer):
-        keep = state
-        for p in range(planes):
-            if p:
-                keep = jnp.where(place == p, state, keep)
-            state = dot3(state, widen(held[p, block, :head_size])) + held[p, block, head_size:]
+        total, keep = held[0, block], nothing
+        for p in range(1, planes):
+            keep = jnp.where(place == p, total, keep)
+            total = compose(total, held[p, block])
+        before.append(keep)
+        whole.append(total)
+    state = jnp.zeros((width, width), jnp.float32)
+    for block in range(outer):
         cut = slice(block * rows, (block + 1) * rows)
-        full = local_ref[cut] + dot3t(carried_ref[cut], widen(keep))
-        centred = full - exact(full, average)
-        variance = exact(centred * centred, average)
+        full = local_ref[cut] + dot3(carried_ref[cut], state_matrix(compose(state, before[block])))
+        if block + 1 < outer:
+            state = compose(state, whole[block])
+        centred = full - spread_sum(full, average)
+        variance = spread_sum(centred * centred, average)
         mixed_ref[cut] = (centred * lax.rsqrt(variance + GROUP_EPSILON) * gain_ref[...]).astype(jnp.bfloat16)
 
     for step in range(planes - 1):
@@ -869,41 +1009,172 @@
     )(state_mixed, conv_mixed, matrix)
 
 
-def delta_blocks_kernel(head_size, chunk, block, *refs):
-    ins, (local_ref, carried_ref, pair_ref), scratch = refs[:7], refs[7:10], refs[10]
-    delta_kernel(head_size, chunk, block, *ins, local_ref, carried_ref, scratch)
-    width = scratch.shape[-1]
-    for first in range(2):
-        total = jnp.zeros((head_size, width), jnp.float32)
-        for h in range(width // head_size):
-            at = first * width + h * head_size
-            total = total + scratch[0, at : at + head_size]
-        pair_ref[0, first * head_size : (first + 1) * head_size] = total
-
-
-def delta_blocks(query, key, value, decay_pre, rate_pre, factor, share, blocks, head_size):
-    total, width = query.shape
-    rows, heads = total // blocks, factor.shape[1]
-    block = math.gcd(rows, 128)
-    chunk = math.gcd(block, 16)
-    wide = pl.BlockSpec((rows, width), lambda i: (i, 0))
-    thin = pl.BlockSpec((rows, heads), lambda i: (i, 0))
-    return pl.pallas_call(
-        functools.partial(delta_blocks_kernel, head_size, chunk, block),
-        grid=(blocks,),
-        in_specs=[wide] * 5 + [thin] * 2,
-        out_specs=[wide, wide, pl.BlockSpec((1, 2 * head_size, width), lambda i: (i, 0, 0))],
-        out_shape=[
-            jax.ShapeDtypeStruct((total, width), jnp.float32),
-            jax.ShapeDtypeStruct((total, width), jnp.float32),
-            jax.ShapeDtypeStruct((blocks, 2 * head_size, width), jnp.float32),
-        ],
-        scratch_shapes=[pltpu.VMEM((1, 2 * width, width), jnp.float32)],
-        cost_estimate=pl.CostEstimate(
-            flops=total * width * width * 60, bytes_accessed=total * width * 32, transcendentals=total * width * 10
-        ),
-        name="delta_chunks",
-    )(query, key, value, decay_pre, rate_pre, factor, share)
+def dotp(left, right, passes, dims=((1,), (0,))):
+    def one(p, q):
+        return lax.dot_general(p, q, (dims, ((), ())), preferred_element_type=jnp.float32)
+
+    if passes == 1:
+        return one(left.astype(jnp.bfloat16), right.astype(jnp.bfloat16))
+    (lh, ll), (rh, rl) = split(left), split(right)
+    return one(lh, rh) + (one(lh, rl) + one(ll, rh))
+
+
+GRID_PASSES, SOLVE_PASSES, SEEN_PASSES, STEP_PASSES, CHAIN_PASSES, READ_PASSES = 3, 3, 3, 3, 3, 3
+
+
+def delta_phases(
+    z, head_size, chunk, block,
+    proj_ref, side_ref, decay_ref, rate_ref, decay_offset_ref, rate_offset_ref,
+    local_ref, carried_ref, pair_ref,
+    mats, adds, hist, queries,
+):
+    groups, _, rows = side_ref.shape
+    width = local_ref.shape[1]
+    heads = side_ref.shape[1] // 2
+    per, pieces = width // head_size, rows // block
+    chunks, steps = block // chunk, rows // chunk
+    wide = per * block
+
+    def iota(shape, dim):
+        return lax.broadcasted_iota(jnp.int32, shape, dim)
+
+    lane_head = iota((1, width), 1) // head_size
+    lane_head2 = (iota((1, 2 * width), 1) % width) // head_size
+    row_w, col_w = iota((width, width), 0), iota((width, width), 1)
+    same_head = (row_w // head_size) == (col_w // head_size)
+    ones_head = jnp.where(same_head, 1.0, 0.0).astype(jnp.bfloat16)
+    row_b, col_b = iota((block, block), 0), iota((block, block), 1)
+    same_chunk = (row_b // chunk) == (col_b // chunk)
+    strict = same_chunk & (row_b > col_b)
+    incl = same_chunk & (row_b >= col_b)
+    sums = jnp.concatenate([jnp.where(incl, 1.0, 0.0), jnp.where(same_chunk, 1.0, 0.0)], axis=0).astype(jnp.bfloat16)
+    row_c, col_c = iota((chunk, wide), 0), iota((chunk, wide), 1) % chunk
+    eye_c = jnp.where(row_c == col_c, 1.0, 0.0)
+    diagonal = (iota((wide, wide), 0) // chunk) == (iota((wide, wide), 1) // chunk)
+    spread_rows = (iota((block, wide), 0) // chunk) == ((iota((block, wide), 1) % block) // chunk)
+    place = iota((2 * heads, 2 * width), 0)
+    chosen = z * per + lane_head2 + jnp.where(iota((1, 2 * width), 1) < width, 0, heads)
+    expand = jnp.where(place == chosen, 1.0, 0.0)
+    ours = pl.ds(pl.multiple_of(z * width, width), width)
+    decay_matrix, rate_matrix = decay_ref[:, ours], rate_ref[:, ours]
+    decay_offset, rate_offset = decay_offset_ref[:, ours], rate_offset_ref[:, ours]
+    side_row = iota((2 * heads, block), 0)
+
+    def by_head(values, mark):
+        return jnp.concatenate([jnp.where(mark == h, values, 0.0) for h in range(per)], axis=0)
+
+    def widen(compact):
+        return jnp.where(diagonal, jnp.concatenate([compact] * (wide // chunk), axis=0), 0.0)
+
+    def one_block(group, piece):
+        start = pl.multiple_of(group * rows + piece * block, block)
+        cut = pl.ds(start, block)
+        here = slice(piece * block, (piece + 1) * block)
+        q, key, v = proj_ref[here, 0:width], proj_ref[here, width : 2 * width], proj_ref[here, 2 * width : 3 * width]
+        inner_width = decay_ref.shape[0]
+        mid_at = 3 * width
+        decay_mid = jnp.tanh(proj_ref[here, mid_at : mid_at + inner_width]).astype(jnp.bfloat16)
+        rate_mid = proj_ref[here, mid_at + inner_width : mid_at + 2 * inner_width].astype(jnp.bfloat16)
+        decay_pre = decay_offset + jnp.dot(decay_mid, decay_matrix, preferred_element_type=jnp.float32)
+        rate_pre = rate_offset + jnp.dot(rate_mid, rate_matrix, preferred_element_type=jnp.float32)
+        thin = side_ref[group, :, piece * block : (piece + 1) * block]
+        thin = jnp.where(side_row < heads, thin, jnp.log(thin))
+        both = lax.dot_general(
+            thin, expand, (((0,), (0,)), ((), ())), precision=HIGHEST, preferred_element_type=jnp.float32
+        )
+        ld = both[:, width:] - (EXP_HALF * jax.nn.sigmoid(decay_pre)) * both[:, :width]
+        learn = jax.nn.sigmoid(rate_pre)
+        unit = key * lax.rsqrt(spread_sum(key * key, ones_head) + UNIT_EPSILON)
+        er, wr = -unit, unit * learn
+        top, rest = split(ld)
+        third = (ld - top.astype(jnp.float32) - rest.astype(jnp.float32)).astype(jnp.bfloat16)
+        both = jnp.dot(sums, top, preferred_element_type=jnp.float32) + (
+            jnp.dot(sums, rest, preferred_element_type=jnp.float32)
+            + jnp.dot(sums, third, preferred_element_type=jnp.float32)
+        )
+        gain, total = both[:block], both[block:]
+        mid = 0.5 * total
+        up, down, bup = jnp.exp(gain - mid), jnp.exp(mid - gain), jnp.exp(gain - ld - mid)
+        left = jnp.concatenate([er * bup, q * up], axis=0)
+        what, khat = wr * down, key * down
+        right = jnp.concatenate(
+            [jnp.where(lane_head == h, item, 0.0) for h in range(per) for item in (what, khat)], axis=0
+        )
+        grid = dotp(left, right, GRID_PASSES, ((1,), (1,)))
+
+        def piece_of(upper, kind, mask):
+            cut_rows = slice(0, block) if upper else slice(block, 2 * block)
+            return jnp.concatenate(
+                [jnp.where(mask, grid[cut_rows, (2 * h + kind) * block : (2 * h + kind + 1) * block], 0.0) for h in range(per)],
+                axis=1,
+            )
+
+        ew, ek = piece_of(True, 0, strict), piece_of(True, 1, strict)
+        rw, rk = piece_of(False, 0, incl), piece_of(False, 1, incl)
+        compact = ew[:chunk]
+        for c in range(1, chunks):
+            compact = compact + ew[c * chunk : (c + 1) * chunk]
+        size = 2
+        inv = eye_c + jnp.where((row_c // size == col_c // size) & (row_c > col_c), compact, 0.0)
+        while size < chunk:
+            off = (row_c // (2 * size) == col_c // (2 * size)) & (row_c // size > col_c // size)
+            part = dotp(inv, widen(jnp.where(off, compact, 0.0)), SOLVE_PASSES)
+            inv = inv + dotp(part, widen(inv), SOLVE_PASSES)
+            size *= 2
+        inverse = jnp.where(spread_rows, jnp.concatenate([inv] * chunks, axis=0), 0.0)
+        seen = dotp(jnp.concatenate([ek, rk], axis=0), by_head(v, lane_head), SEEN_PASSES)
+        eh_full = er * jnp.exp(gain - ld)
+        both = jnp.concatenate([seen[:block], eh_full], axis=1)
+        both = dotp(inverse, by_head(both, lane_head2), SEEN_PASSES)
+        read = dotp(rw, by_head(both, lane_head2), SEEN_PASSES)
+        local_ref[cut] = read[:, :width] + seen[block:]
+        queries[cut] = q * jnp.exp(gain) + read[:, width:]
+        to_end, ends = jnp.exp(total - gain), jnp.exp(total)
+        wend, kend = wr * to_end, key * to_end
+        zero = jnp.zeros((chunk, width), jnp.float32)
+        for c in range(chunks):
+            now = slice(c * chunk, (c + 1) * chunk)
+            lhs = jnp.concatenate([wend[now], kend[now]], axis=0)
+            rhs = jnp.concatenate(
+                [
+                    jnp.concatenate([both[now, width:], both[now, :width]], axis=1),
+                    jnp.concatenate([zero, v[now]], axis=1),
+                ],
+                axis=0,
+            )
+            made = dotp(lhs, rhs, STEP_PASSES, ((0,), (0,)))
+            number = group * steps + piece * chunks + c
+            step = jnp.where(same_head, made[:, :width], 0.0)
+            mats[number] = step + jnp.where(row_w == col_w, ends[c * chunk : c * chunk + 1], 0.0)
+            added = made[:, width:]
+            added = jnp.where(row_w < head_size, pltpu.roll(added, head_size, 1), added)
+            adds[number] = jnp.where(col_w < head_size, 0.0, added)
+
+    begin = jnp.where(row_w % head_size == col_w, 1.0, 0.0)
+
+    def one_step(step, carry):
+        for group in range(groups):
+            number = group * steps + step
+            state = pair_ref[group]
+            hist[number] = state
+            pair_ref[group] = dotp(mats[number], state, CHAIN_PASSES) + adds[number]
+        return carry
+
+    def chain():
+        for group in range(groups):
+            pair_ref[group] = begin
+        lax.fori_loop(0, steps, one_step, 0)
+
+    def one_read(group, carry):
+        for step in range(steps):
+            place_rows = pl.ds(pl.multiple_of(group * rows + step * chunk, chunk), chunk)
+            got = dotp(by_head(queries[place_rows], lane_head), hist[group * steps + step], READ_PASSES)
+            upper, lower = got[:chunk], got[chunk:]
+            carried_ref[place_rows] = jnp.where(lane_head == 0, upper, pltpu.roll(lower, head_size, 1))
+            local_ref[place_rows] += jnp.where(lane_head == 0, pltpu.roll(upper, head_size, 1), lower)
+        return carry
+
+    return one_block, chain, lambda: lax.fori_loop(0, groups, one_read, 0)
 
 
 def body(*args):
@@ -911,7 +1182,7 @@
     heads, channels = args[13].shape[1], args[2].shape[1]
     width = channels // outer
     fits = (
-        lax.axis_size("tp") == 2 and outer > 1 and middle == 2 and inner == 2
+        lax.axis_size("tp") == 2 and outer > 3 and middle == 2 and inner == 2
         and heads % outer == 0 and width == 128 and args[5].shape[1] % (128 * outer) == 0
     )
     return fast_body(*args) if fits else plain_body(*args)
@@ -950,37 +1221,22 @@
         size = value.shape[axis] // outer
         return lax.dynamic_slice_in_dim(value, z * size, size, axis)
 
-    widened = tokens.astype(jnp.float32)
-    normed = (
-        widened
-        * lax.rsqrt(jnp.mean(widened * widened, axis=-1, keepdims=True) + RMS_EPSILON)
-        * input_norm_gain
-    ).astype(jnp.bfloat16)
     side = jnp.concatenate([forgetting_rate_factor.T, state_retention_share.T], axis=0)
     weights = (
         query_matrix, key_matrix, value_matrix, convolution_value_matrix, convolution_gate_matrix,
         attention_output_matrix, convolution_output_matrix,
     )
-    normed, side, (heads_in, conv_in, both_out) = spread(normed, side, weights, ((0, 1, 2), (3, 4), (5, 6)), "sp", "tp")
+    (normed, local, carried, pair), (conv_in, both_out) = spread(
+        tokens, input_norm_gain[None], side, weights, ((0, 1, 2), (3, 4), (5, 6)),
+        (decay_first_matrix, learning_rate_first_matrix),
+        (decay_second_matrix, learning_rate_second_matrix, decay_offset_channel[None], learning_rate_offset[None]),
+        head_size, "sp", "tp",
+    )
     normed = normed.reshape(-1, normed.shape[-1])
 
-    width = channels // outer
-    projected = [
-        jnp.dot(normed, heads_in[:, i * width : (i + 1) * width], preferred_element_type=jnp.float32) for i in range(3)
-    ]
     conv_width = conv_in.shape[1] // 2
     conv_value = jnp.dot(normed, conv_in[:, :conv_width], preferred_element_type=jnp.float32)
     conv_gate = jnp.dot(normed, conv_in[:, conv_width:], preferred_element_type=jnp.float32)
-    decay_mid = jnp.tanh(jnp.dot(normed, decay_first_matrix, preferred_element_type=jnp.float32)).astype(jnp.bfloat16)
-    rate_mid = jnp.dot(normed, learning_rate_first_matrix, preferred_element_type=jnp.float32).astype(jnp.bfloat16)
-    decay_pre = quarter(decay_offset_channel) + jnp.dot(
-        decay_mid, quarter(decay_second_matrix), preferred_element_type=jnp.float32
-    )
-    rate_pre = quarter(learning_rate_offset) + jnp.dot(
-        rate_mid, quarter(learning_rate_second_matrix), preferred_element_type=jnp.float32
-    )
-    few = quarter(side.reshape(outer, 2, heads, rows), 2).transpose(1, 0, 3, 2).reshape(2, outer * rows, heads // outer)
-
     gated = (conv_value * jax.nn.sigmoid(conv_gate)).astype(jnp.bfloat16).reshape(outer, rows, conv_width)
     span = convolution_filter_taps.shape[0]
     ring = [
@@ -997,7 +1253,6 @@
     filtered = filtered.reshape(outer * rows, conv_width)
     sums = jnp.stack([jnp.sum(filtered, axis=-1), jnp.sum(filtered * filtered, axis=-1)])
 
-    local, carried, pair = delta_blocks(*projected, decay_pre, rate_pre, few[0], few[1], outer, head_size)
     state_mixed, totals = states(
         pair, sums, local, carried, quarter(per_head_norm_gain)[None], head_size, "sp", "tp"
     )

time: 261 us -> 193 us (0.74)
  Pallas kernels: 212 us -> 170 us
  matrix products: 22.6 us -> 5.15 us
  local copies, waits for them, and re-layouts: 11.1 us -> 6.52 us
  other arithmetic: 13 us -> 8.98 us
    pallas_call x1 -> x0, Pallas kernels: 56.7 us -> none  [delta_blocks(): pl.pallas_call(functools.partial(delta_blocks_kernel, head_size, chunk, b...]
    dot_general x5 -> x0, matrix products: 17.4 us -> none  [the longest x3 8.52 us: fast_body(): jnp.dot(normed, heads_in[:, i * width:(i + 1) * width], preferred_element...]
    pallas_call x1, Pallas kernels: 88.7 us -> 102 us  [spread(): pl.pallas_call(functools.partial(spread_kernel, axis, pair_axis, radices,...]
  transfers between devices with their start and end apart: 1 -> 1, of which waited for: 0 -> 0; matrix products, arithmetic and copies ran while one was open for 10% -> 2% of each run, Pallas kernels for 22% -> 0%
where the time goes in v2:
time: 193 us
  Pallas kernels  170 us (88%)
  other arithmetic  8.98 us (5%)
  local copies, waits for them, and re-layouts  6.52 us (3%)
  matrix products  5.15 us (3%)
    pallas_call x1, Pallas kernels, spread(): pl.pallas_call(functools.partial(spread_kernel, axis, pair_axis, radices,...  102 us
    pallas_call x1, Pallas kernels, reduce_rows(): pl.pallas_call(functools.partial(reduce_kernel, axis, pair_axis, radices)...  47.5 us
    pallas_call x1, Pallas kernels, states(): pl.pallas_call(functools.partial(states_kernel, axis, pair_axis, radices,...  20.5 us
    reduce_sum x1, other arithmetic, fast_body(): jnp.sum(filtered, axis=-1)  5.06 us
    dot_general x1, matrix products, fast_body(): jnp.dot(normed, conv_in[:, conv_width:], preferred_element_type=jnp.float32)  3.9 us
  transfers between devices with their start and end apart: 1, of which 0 were waited for; matrix products, arithmetic and copies ran while one was open for 2% of the time, Pallas kernels for 0%

profile of v2, /device:TPU:0, one launch (start us, length us, event | category | flops | bytes accessed | tf_op | source)
XLA Modules:
  0.0 193.0 jit_solution(12507016405037845640)
XLA Ops:
  0.0 0.0 copy-start
  0.0 1.3 pad_maximum_fusion.1.refs_2_
  1.3 102.5 %spread_and_delta.1 = (bf16[4,256,2048]{2,1,0:T(8,128)(2,1)}, f32[1024,128]{1,0:T(8,128)}, f32[1024,128]{1,0:T(8,128)}, f32[4,128,128]{2,1,0:T(8,128)}, bf16[4,2...) custom-call(bf16[256,2048]{1,0:T(8,128)(2,1)} %refs_0_.1, f32[1,2048]{1,0:T(1,128)} %bitcast.102, ...), custom_call_target="tpu_custom_call" | custom-call | flops 10000000000 | bytes 16777216 | tf_op jit(solution)/shard_map/spread_and_delta/pallas_call | solution.py:713
  103.8 0.0 copy-start.1
  103.8 0.0 copy-start.2
  103.9 3.9 %fusion.2 = f32[1024,256]{1,0:T(8,128)S(1)} fusion(bf16[1024,2048]{1,0:T(8,128)(2,1)} %bitcast.105, bf16[2048,512]{1,0:T(8,128)(2,1)} %bitcast.107), kind=kOutput, calls=%fused_computation.33 | convolution fusion | flops 1074528256 | bytes 6291456 | tf_op jit(solution)/shard_map/dot_general | solution.py:1239
  107.8 0.0 copy-done.1
  107.8 0.5 copy-done.2
  108.3 1.2 fusion.3
  109.6 1.8 collective-permute-start
  111.3 0.8 dynamic_slice.11
  112.1 1.1 fusion.38
  113.2 1.3 constant_dynamic-slice_fusion
  114.4 0.0 copy-done
  114.5 0.6 dynamic-slice_bitcast_fusion.gain_ref
  115.0 0.0 collective-permute-done
  115.1 5.1 %fusion.37 = (f32[4,256]{1,0:T(4,128)S(1)}, f32[4,256]{1,0:T(4,128)S(1)}, f32[4,256,256]{2,1,0:T(8,128)S(1)}) fusion(bf16[4,256,256]{2,1,0:T(8,128)(2,1)S(1)} %bitcast.61, f32[256]{0:T(256)S(1)} %bitcast.83, bf16[4,30,256]{2,1,0:T(8,128)(2,1)S(1)} %pad_select_fusion, f32[256]{0:T(256)S(1)} %bitcast.85, f32[256]{0:T(256)S(1)} %bitcast.86, ...), kind=kLoop, calls=%fused_computation.89 | loop fusion | flops 48494592 | bytes 1674240 | tf_op jit(solution)/shard_map/reduce_sum | solution.py:1254
  120.1 0.6 pad_maximum_fusion.2.sums_ref
  120.8 20.5 %carry_states.1 = (bf16[1024,128]{1,0:T(8,128)(2,1)}, f32[2,1024]{1,0:T(2,128)}) custom-call(f32[4,128,128]{2,1,0:T(8,128)} %get-tuple-element.13.pair_ref, f32[2,1024]{1,0:T(2,128)} %pad_maximum_fusion.2.sums_ref, f32[1024,128]{1,0:T(8,128)} %get-tuple-element.16.local_ref, f32[1024,128]{1,0:T(8,128)} %get-tuple-element.17.carried_ref, ...), custom_call_target="tpu_custom_call" | custom-call | flops 1000000000 | bytes 1048576 | tf_op jit(solution)/shard_map/carry_states/pallas_call | solution.py:863
  141.2 0.8 slice_multiply_fusion.1
  142.0 1.2 multiply_convert_fusion.conv_ref
  143.2 47.5 %reduce_rows.1 = bf16[256,2048]{1,0:T(8,128)(2,1)} custom-call(bf16[1024,128]{1,0:T(8,128)(2,1)} %get-tuple-element.18.state_ref, bf16[1024,256]{1,0:T(8,128)(2,1)} %multiply_convert_fusion.conv_ref, bf16[2048,384]{1,0:T(8,128)(2,1)} %bitcast.109), custom_call_target="tpu_custom_call" | custom-call | flops 1000000000 | bytes 6291456 | tf_op jit(solution)/shard_map/reduce_rows/pallas_call | solution.py:988
  190.7 2.3 %copy.24 = bf16[256,2048]{1,0:T(8,128)(2,1)} copy(bf16[256,2048]{1,0:T(8,128)(2,1)} %reduce_rows.1) | data formatting | bytes 2097152
  (6 shorter events, 0.1 us)
Async XLA Ops:
  0.0 114.4 %copy-start = (f32[512]{0:T(512)S(1)}, f32[512]{0:T(512)}, u32[]{:S(2)}) copy-start(f32[512]{0:T(512)} %param.35) | copy-start | bytes 6148
  103.8 3.9 %copy-start.1 = (bf16[4,256,2048]{2,1,0:T(8,128)(2,1)S(1)}, bf16[4,256,2048]{2,1,0:T(8,128)(2,1)}, u32[]{:S(2)}) copy-start(bf16[4,256,2048]{2,1,0:T(8,128)(2,1)} %get-tuple-element.14) | copy-start | bytes 12582916
  103.8 4.4 %copy-start.2 = (bf16[4,2,2,128,512]{4,3,2,1,0:T(8,128)(2,1)S(1)}, bf16[4,2,2,128,512]{4,3,2,1,0:T(8,128)(2,1)}, u32[]{:S(2)}) copy-start(bf16[4,2,2,128,512]{4,3,2,1,0:T(8,128)(2,1)} %get-tuple-element.15) | copy-start | bytes 6291460
  109.6 5.5 %collective-permute-start = (bf16[4,30,256]{2,1,0:T(8,128)(2,1)S(1)}, bf16[4,30,256]{2,1,0:T(8,128)(2,1)S(1)}, u32[]{:S(2)}, u32[]{:S(2)}) collective-permute-start(bf16[4,30,256]{2,1,0:T(8,128)(2,1)S(1)} %slice.270), channel_id=1, source_target_pairs={{0,2},{2,4},{4,6},{6,0},{8,10},{10,12},{12,14},{14,8},{16,18},{18,... | collective-permute-start | bytes 184328 | tf_op jit(solution)/shard_map/ppermute | solution.py:1245

commit v3 on v2

--- a/solution.py
+++ b/solution.py
@@ -434,15 +434,15 @@
     number = len(widths)
     raw_ref, gain_ref, side_ref, ins = refs[0], refs[1], refs[2], refs[3 : 3 + number]
     refs = refs[3 + number :]
-    extra, (decay_ref, rate_ref, decay_offset_ref, rate_offset_ref) = refs[: len(firsts)], refs[len(firsts) : len(firsts) + 4]
-    refs = refs[len(firsts) + 4 :]
+    extra, maps, refs = refs[: len(firsts)], refs[len(firsts) : len(firsts) + 7], refs[len(firsts) + 7 :]
+    decay_ref, rate_ref, decay_offset_ref, rate_offset_ref, taps_ref, head_gain_ref, conv_gain_ref = maps
     kinds = 1 + max(out for out, _ in placed)
-    tokens_all, local_ref, carried_ref, pair_ref = refs[:4]
-    later, refs = refs[4 : 3 + kinds], refs[3 + kinds :]
-    (first_out, tokens_out, side_out, tokens_ref, proj, mats, adds, hist, queries,
+    out_ref, local_ref, carried_ref, pair_ref, filtered_ref, stats_ref, last_out = refs[:7]
+    finish_refs, refs = refs[7:27], refs[27:]
+    (first_out, second_out, padded, rim_out, rim_in, rim_send, rim_recv, tokens_out, side_out, tokens_ref, proj, mats, adds, hist, queries,
      first_sem, own_sem, far_send, far_recv, near_send, near_recv, side_send, side_recv,
      tok_send, tok_recv, sib_send, sib_recv) = refs
-    outs = [first_out, *later]
+    outs = [first_out, second_out, last_out]
     outer, middle, inner = radices
     z, y, x = place_of(axis, radices)
     core = lax.axis_index(pair_axis)
@@ -457,11 +457,14 @@
 
     far = [(z + step) % outer for step in range(1, outer)]
     near = {"x": index(z, y, 1 - x), "y": index(z, 1 - y, x)}
-    greet(
-        [{axis: index(at, y, x)} for at in far]
-        + [{axis: peer} for peer in near.values()]
-        + [{pair_axis: 1 - core}]
-    )
+    planes = middle * inner
+    plane = y * inner + x
+    peers, send_pairs, send_stats, wait_pairs, make_states, state_rows, wait_stats, reduce_all = finish_phases(
+        axis, pair_axis, radices, head_size,
+        pair_ref, stats_ref, local_ref, carried_ref, head_gain_ref, filtered_ref, conv_gain_ref, last_out, out_ref,
+        *finish_refs,
+    )
+    greet(peers)
 
     def part(w, at):
         return ins[w].at[:, pl.ds(pl.multiple_of(at * widths[w], widths[w]), widths[w])]
@@ -548,6 +551,8 @@
         @pl.when(sends(way, 0))
         def _():
             token_copy(way, 0, z, tokens_ref.at[mine]).start()
+    rest = [[w for w in range(number) if placed[w][0] == out] for out in range(1, kinds)]
+    send_far(rest[0])
     own[number].start()
     own[number + 1].start()
     kept = []
@@ -606,7 +611,9 @@
     for step in range(outer - 1):
         side_copy(step, far[step], (z + outer - step - 1) % outer).wait_recv()
     token_step(0)
-    rest = [[w for w in range(number) if placed[w][0] == out] for out in range(1, kinds)]
+    send_far(rest[1])
+    for w in rest[0]:
+        advance(w, 0)
     one_block, chain, read = delta_phases(
         z, head_size, chunk, block, proj, side_out, decay_ref, rate_ref, decay_offset_ref, rate_offset_ref,
         local_ref, carried_ref, pair_ref, mats, adds, hist, queries,
@@ -641,36 +648,102 @@
         for piece in range(pieces):
             one_block(group, piece)
             if piece == 0:
+                @pl.when(k == 0)
+                def _():
+                    for w in rest[0]:
+                        advance(w, 1)
+
+                @pl.when(k == 2)
+                def _():
+                    for w in rest[1]:
+                        advance(w, 1)
+
                 @pl.when((k > 0) & (k < outer - 1))
                 def _():
                     token_step(k)
 
-                for at, some in enumerate(rest):
-                    @pl.when(k == at)
-                    def _():
-                        send_far(some)
-
-                    for stage in range(last):
-                        @pl.when(k == at + 2 + stage)
-                        def _():
-                            for w in some:
-                                advance(w, stage)
+                @pl.when(k == 1)
+                def _():
+                    for w in rest[1]:
+                        advance(w, 0)
         return carry
 
     lax.fori_loop(0, outer, one_round, 0)
-    keep_tokens = pltpu.make_async_copy(tokens_out, tokens_all, own_sem.at[number + 2])
-    keep_tokens.start()
     chain()
-    for at, some in enumerate(rest):
-        for stage in range(last + 1):
-            if at + 2 + stage >= outer and stage < last:
-                for w in some:
-                    advance(w, stage)
+
+    rows = tokens_ref.shape[0]
+    span, rim_rows = taps_ref.shape[0], rim_out.shape[1]
+    conv_width = second_out.shape[-1] // 2
+    for w in rest[0]:
+        advance(w, last)
+
+    def gate(group, carry):
+        total = None
+        for part_at in range(outer):
+            matrix = second_out[part_at].reshape(piece_depth, 2 * conv_width)
+            term = jnp.dot(
+                tokens_out[group, :, part_at * piece_depth : (part_at + 1) * piece_depth], matrix,
+                preferred_element_type=jnp.float32,
+            )
+            total = term if total is None else total + term
+        gated = (total[:, :conv_width] * jax.nn.sigmoid(total[:, conv_width:])).astype(jnp.bfloat16)
+        padded[group, rim_rows:] = gated.astype(jnp.float32)
+        rim_out[group] = gated[rows - rim_rows :]
+        return carry
+
+    lax.fori_loop(0, outer, gate, 0)
+    rim_copy = pltpu.make_async_remote_copy(
+        src_ref=rim_out, dst_ref=rim_in, send_sem=rim_send.at[0], recv_sem=rim_recv.at[0],
+        device_id={axis: z * planes + (plane + 1) % planes}, device_id_type=MESH,
+    )
+    rim_copy.start()
+    send_pairs()
     read()
-    for some in rest:
-        for w in some:
-            advance(w, last)
-    keep_tokens.wait()
+    rim_copy.wait_recv()
+    for group in range(outer):
+        before = jnp.zeros(rim_in.shape[1:], jnp.bfloat16) if group == 0 else rim_in[group - 1]
+        padded[group, :rim_rows] = jnp.where(plane == 0, before, rim_in[group]).astype(jnp.float32)
+    taps = taps_ref[:, pl.ds(pl.multiple_of(z * conv_width, conv_width), conv_width)]
+    part_rows = math.gcd(rows, 64)
+    row_8 = lax.broadcasted_iota(jnp.int32, (8, conv_width), 0)
+    sum_rows = [jnp.where(row_8 == at, 1.0, 0.0).astype(jnp.bfloat16) for at in range(2)]
+    skip = rim_rows - (span - 1)
+
+    def row_sums(values, marks):
+        total = None
+        for _ in range(3):
+            top = values.astype(jnp.bfloat16)
+            term = lax.dot_general(marks, top, (((1,), (1,)), ((), ())), preferred_element_type=jnp.float32)
+            total = term if total is None else total + term
+            values = values - top.astype(jnp.float32)
+        return total
+
+    def convolve(number, carry):
+        group, start = number // (rows // part_rows), (number % (rows // part_rows)) * part_rows
+        window = padded[group, pl.ds(pl.multiple_of(start, part_rows), part_rows + rim_rows)]
+        total = jnp.zeros((part_rows, conv_width), jnp.float32)
+        for turn in range(8):
+            moved = window if turn == 0 else window[turn : turn + part_rows + rim_rows - 8]
+            for tap in range(span):
+                if (tap + skip) % 8 == turn:
+                    first = tap + skip - turn
+                    total = total + taps[tap : tap + 1] * moved[first : first + part_rows]
+        filtered_ref[pl.ds(pl.multiple_of(number * part_rows, part_rows), part_rows)] = total
+        return carry
+
+    lax.fori_loop(0, outer * (rows // part_rows), convolve, 0)
+    for group in range(outer):
+        values = filtered_ref[group * rows : (group + 1) * rows]
+        stats_ref[group] = row_sums(values, sum_rows[0]) + row_sums(values * values, sum_rows[1])
+    for w in rest[1]:
+        advance(w, last)
+    send_stats()
+    wait_pairs()
+    make_states()
+    state_rows()
+    wait_stats()
+    reduce_all()
+    rim_copy.wait_send()
     for step in range(outer - 1):
         side_copy(step, far[step], z).wait_send()
     for step in range(outer - 1):
@@ -709,22 +782,42 @@
     block = math.gcd(rows, 128)
     chunk = math.gcd(block, 32)
     total = outer * rows
-    vmem, hbm = pl.BlockSpec(memory_space=pltpu.VMEM), pl.BlockSpec(memory_space=pl.ANY)
-    outs = pl.pallas_call(
+    conv_width, rim_rows = totals[1] // 2, -(-(maps[4].shape[0] - 1) // 16) * 16
+    vmem, dma = pl.BlockSpec(memory_space=pltpu.VMEM), pltpu.SemaphoreType.DMA
+    planes, lines = radices[1] * radices[2], outer * lax.axis_size(pair_axis) - 1
+    half, slots = tokens.shape[1] // 2, (2, outer - 1)
+    return pl.pallas_call(
         functools.partial(
             spread_kernel, axis, pair_axis, radices, widths, placed, extras, groups[0], head_size, chunk, block
         ),
         in_specs=[vmem] * (3 + number + len(firsts) + len(maps)),
-        out_specs=[hbm] + [vmem] * 3 + [hbm] * (len(groups) - 1),
-        out_shape=[
-            jax.ShapeDtypeStruct((outer,) + tokens.shape, tokens.dtype),
-            jax.ShapeDtypeStruct((total, width), jnp.float32),
-            jax.ShapeDtypeStruct((total, width), jnp.float32),
-            jax.ShapeDtypeStruct((outer, width, width), jnp.float32),
-        ]
-        + [jax.ShapeDtypeStruct(radices + (depth, size), weights[0].dtype) for size in totals[1:]],
+        out_specs=vmem,
+        out_shape=jax.ShapeDtypeStruct(tokens.shape, jnp.bfloat16),
         scratch_shapes=[
+            pltpu.VMEM((total, width), jnp.float32),
+            pltpu.VMEM((total, width), jnp.float32),
+            pltpu.VMEM((outer, width, width), jnp.float32),
+            pltpu.VMEM((total, conv_width), jnp.float32),
+            pltpu.VMEM((outer, 8, rows), jnp.float32),
+            pltpu.VMEM(radices + (depth, totals[2]), weights[0].dtype),
+            pltpu.VMEM((planes, outer, width, width), jnp.float32),
+            pltpu.VMEM((lines, outer, 8, rows), jnp.float32),
+            pltpu.VMEM((outer, width, width), jnp.float32),
+            pltpu.VMEM((outer, rows, width + conv_width), jnp.bfloat16),
+            pltpu.VMEM((outer, rows, half), jnp.float32),
+            pltpu.VMEM((outer, rows, half), jnp.bfloat16),
+            pltpu.VMEM((outer, rows, half), jnp.bfloat16),
+            pltpu.VMEM(slots + (rows, half), jnp.bfloat16),
+            pltpu.VMEM(slots + (rows, half), jnp.bfloat16),
+            dma((1,)), dma((planes - 1,)), dma((planes - 1,)), dma((lines,)), dma((lines,)),
+            dma((outer,)), dma((outer,)), dma(slots), dma(slots), dma((1,)), dma((1,)),
             pltpu.VMEM(radices + (depth, totals[0]), weights[0].dtype),
+            pltpu.VMEM(radices + (depth, totals[1]), weights[0].dtype),
+            pltpu.VMEM((outer, rim_rows + rows, conv_width), jnp.float32),
+            pltpu.VMEM((outer, rim_rows, conv_width), weights[0].dtype),
+            pltpu.VMEM((outer, rim_rows, conv_width), weights[0].dtype),
+            pltpu.SemaphoreType.DMA((1,)),
+            pltpu.SemaphoreType.DMA((1,)),
             pltpu.VMEM((outer,) + tokens.shape, tokens.dtype),
             pltpu.VMEM((outer,) + side.shape, side.dtype),
             pltpu.VMEM(tokens.shape, tokens.dtype),
@@ -748,9 +841,8 @@
         ],
         compiler_params=pltpu.CompilerParams(collective_id=0, has_side_effects=True, vmem_limit_bytes=60 * 2**20),
         cost_estimate=pl.CostEstimate(flops=10**10, bytes_accessed=8 * tokens.size * outer, transcendentals=0),
-        name="spread_and_delta",
+        name="whole_layer",
     )(tokens, gain, side, *weights, *firsts, *maps)
-    return outs[:4], [out.reshape(-1, size) for out, size in zip(outs[4:], totals[1:])]
 
 
 def spread_sum(values, matrix):
@@ -760,19 +852,22 @@
     )
 
 
-def states_kernel(
+def finish_phases(
     axis, pair_axis, radices, head_size,
-    pair_ref, sums_ref, local_ref, carried_ref, gain_ref,
-    mixed_ref, totals_ref,
-    held, stats, own_sem, pair_send, pair_recv, stat_send, stat_recv,
+    pair_ref, stats_ref, local_ref, carried_ref, gain_ref, filtered_ref, conv_gain_ref, matrix_ref,
+    out_ref,
+    held, stats, smat, mixed_all, keep, twin_out, twin_in, chain_out, chain_in,
+    own_sem, pair_send, pair_recv, stat_send, stat_recv,
+    twin_send, twin_recv, chain_send, chain_recv, last_send, last_recv,
 ):
     outer, middle, inner = radices
     planes = middle * inner
     z, y, x = place_of(axis, radices)
     place = y * inner + x
     core = lax.axis_index(pair_axis)
-    width = pair_ref.shape[-1]
-    rows = local_ref.shape[0] // outer
+    width, conv_width = pair_ref.shape[-1], filtered_ref.shape[-1]
+    rows, half = keep.shape[1:]
+    ways = (1, -1)
     plane_peers = [(place + step) % planes for step in range(1, planes)]
     cores = lax.axis_size(pair_axis)
     lines = [(dz, dc) for dz in range(outer) for dc in range(cores) if dz or dc]
@@ -780,7 +875,10 @@
     def line_device(dz, dc):
         return {axis: ((z + dz) % outer) * planes + place, pair_axis: (core + dc) % cores}
 
-    greet([{axis: z * planes + peer} for peer in plane_peers] + [line_device(*line) for line in lines])
+    def inside(at):
+        return (at >= 0) & (at < outer)
+
+    peers = [{axis: z * planes + peer} for peer in plane_peers] + [line_device(*line) for line in lines]
 
     def pair_copy(step, p_from):
         return pltpu.make_async_remote_copy(
@@ -789,117 +887,12 @@
             device_id={axis: z * planes + plane_peers[step]}, device_id_type=MESH,
         )
 
-    def stat_copy(number, slot):
+    def stat_copy(number):
         return pltpu.make_async_remote_copy(
-            src_ref=sums_ref, dst_ref=stats.at[slot],
+            src_ref=stats_ref, dst_ref=stats.at[number],
             send_sem=stat_send.at[number], recv_sem=stat_recv.at[number],
             device_id=line_device(*lines[number]), device_id_type=MESH,
         )
-
-    for step in range(planes - 1):
-        pair_copy(step, place).start()
-    for number in range(len(lines)):
-        stat_copy(number, number).start()
-    own = pltpu.make_async_copy(pair_ref, held.at[place], own_sem.at[0])
-    own.start()
-
-    for number in range(len(lines)):
-        stat_copy(number, number).wait_recv()
-    totals = sums_ref[...]
-    for number in range(len(lines)):
-        totals = totals + stats[number]
-    totals_ref[...] = totals
-
-    own.wait()
-    for step in range(planes - 1):
-        pair_copy(step, (place + planes - step - 1) % planes).wait_recv()
-
-    row = lax.broadcasted_iota(jnp.int32, (width, width), 0)
-    lane = lax.broadcasted_iota(jnp.int32, (width, width), 1)
-    average = jnp.where((row // head_size) == (lane // head_size), 1.0 / head_size, 0.0).astype(jnp.bfloat16)
-    first_head, moves = row < head_size, lane < head_size
-
-    def step_matrix(item):
-        part = jnp.where(moves, item, 0.0)
-        return jnp.where(first_head, part, pltpu.roll(part, head_size, 1))
-
-    def state_matrix(item):
-        part = jnp.where(moves, 0.0, item)
-        return jnp.where(first_head, pltpu.roll(part, head_size, 1), part)
-
-    def compose(earlier, later):
-        return dot3(step_matrix(later), earlier) + jnp.where(moves, 0.0, later)
-
-    nothing = jnp.where(moves & (row % head_size == lane), 1.0, 0.0)
-    before, whole = [], []
-    for block in range(outer):
-        total, keep = held[0, block], nothing
-        for p in range(1, planes):
-            keep = jnp.where(place == p, total, keep)
-            total = compose(total, held[p, block])
-        before.append(keep)
-        whole.append(total)
-    state = jnp.zeros((width, width), jnp.float32)
-    for block in range(outer):
-        cut = slice(block * rows, (block + 1) * rows)
-        full = local_ref[cut] + dot3(carried_ref[cut], state_matrix(compose(state, before[block])))
-        if block + 1 < outer:
-            state = compose(state, whole[block])
-        centred = full - spread_sum(full, average)
-        variance = spread_sum(centred * centred, average)
-        mixed_ref[cut] = (centred * lax.rsqrt(variance + GROUP_EPSILON) * gain_ref[...]).astype(jnp.bfloat16)
-
-    for step in range(planes - 1):
-        pair_copy(step, place).wait_send()
-    for number in range(len(lines)):
-        stat_copy(number, number).wait_send()
-
-
-def states(pair, sums, local, carried, gain, head_size, axis, pair_axis):
-    radices = radices_of(axis)
-    planes, cores = radices[1] * radices[2], lax.axis_size(pair_axis)
-    lines = radices[0] * cores - 1
-    vmem = pl.BlockSpec(memory_space=pltpu.VMEM)
-    return pl.pallas_call(
-        functools.partial(states_kernel, axis, pair_axis, radices, head_size),
-        in_specs=[vmem] * 5,
-        out_specs=[vmem] * 2,
-        out_shape=[jax.ShapeDtypeStruct(local.shape, jnp.bfloat16), jax.ShapeDtypeStruct(sums.shape, jnp.float32)],
-        scratch_shapes=[
-            pltpu.VMEM((planes,) + pair.shape, jnp.float32),
-            pltpu.VMEM((lines,) + sums.shape, jnp.float32),
-            pltpu.SemaphoreType.DMA((1,)),
-            pltpu.SemaphoreType.DMA((planes - 1,)),
-            pltpu.SemaphoreType.DMA((planes - 1,)),
-            pltpu.SemaphoreType.DMA((lines,)),
-            pltpu.SemaphoreType.DMA((lines,)),
-        ],
-        compiler_params=pltpu.CompilerParams(collective_id=1, has_side_effects=True),
-        cost_estimate=pl.CostEstimate(flops=10**9, bytes_accessed=pair.size * 16, transcendentals=0),
-        name="carry_states",
-    )(pair, sums, local, carried, gain)
-
-
-def reduce_kernel(
-    axis, pair_axis, radices,
-    state_ref, conv_ref, matrix_ref, out_ref,
-    keep, twin_out, twin_in, chain_out, chain_in,
-    twin_send, twin_recv, chain_send, chain_recv, last_send, last_recv,
-):
-    outer, middle, inner = radices
-    z, y, x = place_of(axis, radices)
-    core = lax.axis_index(pair_axis)
-    rows, half = keep.shape[1:]
-    split_at = state_ref.shape[1]
-    ways = (1, -1)
-
-    def index(z_at):
-        return (z_at * middle + y) * inner + x
-
-    def inside(at):
-        return (at >= 0) & (at < outer)
-
-    greet([{axis: index((z + step) % outer)} for step in range(1, outer)] + [{pair_axis: 1 - core}])
 
     def twin_copy(block):
         return pltpu.make_async_remote_copy(
@@ -912,101 +905,177 @@
         return pltpu.make_async_remote_copy(
             src_ref=chain_out.at[way, steps - 1], dst_ref=chain_in.at[way, steps - 1],
             send_sem=chain_send.at[way, steps - 1], recv_sem=chain_recv.at[way, steps - 1],
-            device_id={axis: index((z + ways[way] + outer) % outer)}, device_id_type=MESH,
-        )
+            device_id={axis: ((z + 1 - 2 * way + outer) % outer) * planes + place}, device_id_type=MESH,
+        )
+
+    own = pltpu.make_async_copy(pair_ref, held.at[place], own_sem.at[0])
+
+    def send_pairs():
+        for step in range(planes - 1):
+            pair_copy(step, place).start()
+        own.start()
+
+    def send_stats():
+        for number in range(len(lines)):
+            stat_copy(number).start()
+
+    channels = conv_width * outer * cores
+    conv_gain = conv_gain_ref[:, pl.ds(pl.multiple_of(z * conv_width, conv_width), conv_width)]
+    lane_2 = lax.broadcasted_iota(jnp.int32, (8, 256), 1) // 128
+    pick = jnp.where(lax.broadcasted_iota(jnp.int32, (8, 256), 0) == lane_2, 1.0, 0.0)
+    dims = (((1,), (1,)), ((), ()))
+
+    def rows_of(block):
+        return pl.ds(pl.multiple_of(block * rows, rows), rows)
+
+    def side_rows(side):
+        return pl.ds(pl.multiple_of(side * half, half), half)
+
+    def side_matrix(side):
+        these = matrix_ref[pl.ds(side * (outer // 2), outer // 2)]
+        return these.reshape(half, matrix_ref.shape[-1])
+
+    def conv_part(block):
+        totals = stats_ref[block]
+        for number in range(len(lines)):
+            totals = totals + stats[number, block]
+        spread_totals = lax.dot_general(
+            totals, pick, (((0,), (0,)), ((), ())), precision=HIGHEST, preferred_element_type=jnp.float32
+        )
+        mean, square = spread_totals[:, :128] / channels, spread_totals[:, 128:] / channels
+        scale = lax.rsqrt(square - mean * mean + LAYER_EPSILON)
+        mean = jnp.concatenate([mean] * (conv_width // 128), axis=1)
+        scale = jnp.concatenate([scale] * (conv_width // 128), axis=1)
+        normal = (filtered_ref[rows_of(block), :] - mean) * scale * conv_gain
+        mixed_all[block, :, width:] = jax.nn.silu(normal).astype(jnp.bfloat16)
+
+    row = lax.broadcasted_iota(jnp.int32, (width, width), 0)
+    lane = lax.broadcasted_iota(jnp.int32, (width, width), 1)
+    average = jnp.where((row // head_size) == (lane // head_size), 1.0 / head_size, 0.0).astype(jnp.bfloat16)
+    first_head, moves = row < head_size, lane < head_size
+
+    def step_matrix(item):
+        part = jnp.where(moves, item, 0.0)
+        return jnp.where(first_head, part, pltpu.roll(part, head_size, 1))
+
+    def state_matrix(item):
+        part = jnp.where(moves, 0.0, item)
+        return jnp.where(first_head, pltpu.roll(part, head_size, 1), part)
+
+    def compose(earlier, later):
+        return dot3(step_matrix(later), earlier) + jnp.where(moves, 0.0, later)
+
+    nothing = jnp.where(moves & (row % head_size == lane), 1.0, 0.0)
+
+    def wait_pairs():
+        own.wait()
+        for step in range(planes - 1):
+            pair_copy(step, (place + planes - step - 1) % planes).wait_recv()
+
+    def make_states():
+        before, whole = [], []
+        for block in range(outer):
+            total, kept = held[0, block], nothing
+            for p in range(1, planes):
+                kept = jnp.where(place == p, total, kept)
+                total = compose(total, held[p, block])
+            before.append(kept)
+            whole.append(total)
+        state = jnp.zeros((width, width), jnp.float32)
+        for block in range(outer):
+            smat[block] = state_matrix(compose(state, before[block]))
+            if block + 1 < outer:
+                state = compose(state, whole[block])
+
+    gain = gain_ref[:, pl.ds(pl.multiple_of(z * width, width), width)]
+
+    def state_part(block, carry):
+        cut = rows_of(block)
+        full = local_ref[cut, :] + dot3(carried_ref[cut, :], smat[block])
+        centred = full - spread_sum(full, average)
+        variance = spread_sum(centred * centred, average)
+        mixed_all[block, :, :width] = (centred * lax.rsqrt(variance + GROUP_EPSILON) * gain).astype(jnp.bfloat16)
+        return carry
+
+    def at_end():
+        return (z == 0) | (z == outer - 1)
+
+    def order(number):
+        return jnp.where(z < outer // 2, outer - 1 - number, number)
 
     def product(block, side):
-        cut = pl.ds(pl.multiple_of(block * rows, rows), rows)
-        these = pl.ds(pl.multiple_of(side * half, half), half)
-        dims = (((1,), (1,)), ((), ()))
         return lax.dot_general(
-            state_ref[cut, :], matrix_ref[these, :split_at], dims, preferred_element_type=jnp.float32
-        ) + lax.dot_general(
-            conv_ref[cut, :], matrix_ref[these, split_at:], dims, preferred_element_type=jnp.float32
-        )
-
-    def one_block(number, carry):
-        block = jnp.where(z < outer // 2, outer - 1 - number, number)
+            mixed_all[block], side_matrix(side), dims, preferred_element_type=jnp.float32
+        )
+
+    def one_product(number, carry):
+        block = order(number)
+        conv_part(block)
         twin_out[block] = product(block, 1 - core).astype(jnp.bfloat16)
         twin_copy(block).start()
         keep[block] = product(block, core)
+
+        @pl.when(at_end() & (number > 0))
+        def _():
+            earlier = order(number - 1)
+            way = jnp.where(z == 0, 0, 1)
+            steps = jnp.where(z == 0, earlier, z - earlier)
+            twin_copy(earlier).wait_recv()
+            chain_out[way, steps - 1] = (keep[earlier] + twin_in[earlier].astype(jnp.float32)).astype(jnp.bfloat16)
+            chain_copy(way, steps).start()
         return carry
 
-    lax.fori_loop(0, outer, one_block, 0)
-
-    for steps in range(outer - 1, 0, -1):
+    def wait_stats():
+        for number in range(len(lines)):
+            stat_copy(number).wait_recv()
+
+    def reduce_all():
+        lax.fori_loop(0, outer, one_product, 0)
+        for steps in range(outer - 2, 0, -1):
+            for way in range(2):
+                block = z + ways[way] * steps
+
+                @pl.when(inside(block) & (z > 0) & (z < outer - 1))
+                def _():
+                    twin_copy(block).wait_recv()
+                    keep[block] += twin_in[block].astype(jnp.float32)
+                    chain_copy(way, steps + 1).wait_recv()
+                    chain_out[way, steps - 1] = (keep[block] + chain_in[way, steps].astype(jnp.float32)).astype(jnp.bfloat16)
+                    chain_copy(way, steps).start()
+
+        twin_copy(z).wait_recv()
+        keep[z] += twin_in[z].astype(jnp.float32)
         for way in range(2):
-            block = z + ways[way] * steps
-
-            @pl.when(inside(block))
+            @pl.when(inside(z - ways[way]))
             def _():
-                twin_copy(block).wait_recv()
-                keep[block] += twin_in[block].astype(jnp.float32)
-                if steps + 1 < outer:
-                    @pl.when(inside(z - ways[way]))
-                    def _():
-                        chain_copy(way, steps + 1).wait_recv()
-                        keep[block] += chain_in[way, steps].astype(jnp.float32)
-                chain_out[way, steps - 1] = keep[block].astype(jnp.bfloat16)
-                chain_copy(way, steps).start()
-
-    twin_copy(z).wait_recv()
-    keep[z] += twin_in[z].astype(jnp.float32)
-    for way in range(2):
-        @pl.when(inside(z - ways[way]))
-        def _():
-            chain_copy(way, 1).wait_recv()
-            keep[z] += chain_in[way, 0].astype(jnp.float32)
-
-    ours = pl.ds(pl.multiple_of(core * half, half), half)
-    out_ref[:, ours] = keep[z].astype(jnp.bfloat16)
-
-    def last_copy(side):
-        place = out_ref.at[:, pl.ds(pl.multiple_of(side * half, half), half)]
-        return pltpu.make_async_remote_copy(
-            src_ref=place, dst_ref=place, send_sem=last_send.at[0], recv_sem=last_recv.at[0],
-            device_id={pair_axis: 1 - core}, device_id_type=MESH,
-        )
-
-    last_copy(core).start()
-    for block in range(outer):
-        twin_copy(block).wait_send()
-    for steps in range(outer - 1, 0, -1):
-        for way in range(2):
-            @pl.when(inside(z + ways[way] * steps))
-            def _():
-                chain_copy(way, steps).wait_send()
-    last_copy(1 - core).wait_recv()
-    last_copy(core).wait_send()
-
-
-def reduce_rows(state_mixed, conv_mixed, matrix, outer, axis, pair_axis):
-    radices = radices_of(axis)
-    rows, half = state_mixed.shape[0] // outer, matrix.shape[0] // 2
-    vmem = pl.BlockSpec(memory_space=pltpu.VMEM)
-    slots = (2, outer - 1)
-    return pl.pallas_call(
-        functools.partial(reduce_kernel, axis, pair_axis, radices),
-        in_specs=[vmem] * 3,
-        out_specs=vmem,
-        out_shape=jax.ShapeDtypeStruct((rows, 2 * half), jnp.bfloat16),
-        scratch_shapes=[
-            pltpu.VMEM((outer, rows, half), jnp.float32),
-            pltpu.VMEM((outer, rows, half), jnp.bfloat16),
-            pltpu.VMEM((outer, rows, half), jnp.bfloat16),
-            pltpu.VMEM(slots + (rows, half), jnp.bfloat16),
-            pltpu.VMEM(slots + (rows, half), jnp.bfloat16),
-            pltpu.SemaphoreType.DMA((outer,)),
-            pltpu.SemaphoreType.DMA((outer,)),
-            pltpu.SemaphoreType.DMA(slots),
-            pltpu.SemaphoreType.DMA(slots),
-            pltpu.SemaphoreType.DMA((1,)),
-            pltpu.SemaphoreType.DMA((1,)),
-        ],
-        compiler_params=pltpu.CompilerParams(collective_id=2, has_side_effects=True, vmem_limit_bytes=60 * 2**20),
-        cost_estimate=pl.CostEstimate(flops=10**9, bytes_accessed=matrix.size * 8, transcendentals=0),
-        name="reduce_rows",
-    )(state_mixed, conv_mixed, matrix)
+                chain_copy(way, 1).wait_recv()
+                keep[z] += chain_in[way, 0].astype(jnp.float32)
+
+        out_ref[:, side_rows(core)] = keep[z].astype(jnp.bfloat16)
+
+        def last_copy(side):
+            where = out_ref.at[:, side_rows(side)]
+            return pltpu.make_async_remote_copy(
+                src_ref=where, dst_ref=where, send_sem=last_send.at[0], recv_sem=last_recv.at[0],
+                device_id={pair_axis: 1 - core}, device_id_type=MESH,
+            )
+
+        last_copy(core).start()
+        for step in range(planes - 1):
+            pair_copy(step, place).wait_send()
+        for number in range(len(lines)):
+            stat_copy(number).wait_send()
+        for block in range(outer):
+            twin_copy(block).wait_send()
+        for steps in range(outer - 1, 0, -1):
+            for way in range(2):
+                @pl.when(inside(z + ways[way] * steps))
+                def _():
+                    chain_copy(way, steps).wait_send()
+        last_copy(1 - core).wait_recv()
+        last_copy(core).wait_send()
+
+    return peers, send_pairs, send_stats, wait_pairs, make_states, lambda: lax.fori_loop(0, outer, state_part, 0), wait_stats, reduce_all
 
 
 def dotp(left, right, passes, dims=((1,), (0,))):
@@ -1210,60 +1279,22 @@
     attention_output_matrix,
     convolution_output_matrix,
 ):
-    outer, middle, inner = radices_of("sp")
-    planes = middle * inner
-    rows = tokens.shape[0]
     heads, channels = forgetting_rate_factor.shape[1], query_matrix.shape[1]
     head_size = channels // heads
-    z = lax.axis_index("sp") // planes
-
-    def quarter(value, axis=-1):
-        size = value.shape[axis] // outer
-        return lax.dynamic_slice_in_dim(value, z * size, size, axis)
-
     side = jnp.concatenate([forgetting_rate_factor.T, state_retention_share.T], axis=0)
     weights = (
         query_matrix, key_matrix, value_matrix, convolution_value_matrix, convolution_gate_matrix,
         attention_output_matrix, convolution_output_matrix,
     )
-    (normed, local, carried, pair), (conv_in, both_out) = spread(
+    return spread(
         tokens, input_norm_gain[None], side, weights, ((0, 1, 2), (3, 4), (5, 6)),
         (decay_first_matrix, learning_rate_first_matrix),
-        (decay_second_matrix, learning_rate_second_matrix, decay_offset_channel[None], learning_rate_offset[None]),
+        (
+            decay_second_matrix, learning_rate_second_matrix, decay_offset_channel[None], learning_rate_offset[None],
+            convolution_filter_taps, per_head_norm_gain[None], convolution_channel_gain[None],
+        ),
         head_size, "sp", "tp",
     )
-    normed = normed.reshape(-1, normed.shape[-1])
-
-    conv_width = conv_in.shape[1] // 2
-    conv_value = jnp.dot(normed, conv_in[:, :conv_width], preferred_element_type=jnp.float32)
-    conv_gate = jnp.dot(normed, conv_in[:, conv_width:], preferred_element_type=jnp.float32)
-    gated = (conv_value * jax.nn.sigmoid(conv_gate)).astype(jnp.bfloat16).reshape(outer, rows, conv_width)
-    span = convolution_filter_taps.shape[0]
-    ring = [
-        (at * planes + p, at * planes + (p + 1) % planes) for at in range(outer) for p in range(planes)
-    ]
-    rim = lax.ppermute(gated[:, rows - (span - 1) :], "sp", ring)
-    shifted = jnp.concatenate([jnp.zeros_like(rim[:1]), rim[:-1]], axis=0)
-    rim = jnp.where(lax.axis_index("sp") % planes == 0, shifted, rim)
-    padded = jnp.concatenate([rim, gated], axis=1)
-    taps = quarter(convolution_filter_taps)
-    filtered = jnp.zeros(gated.shape, jnp.float32)
-    for offset in range(span):
-        filtered = filtered + taps[offset] * padded[:, offset : offset + rows]
-    filtered = filtered.reshape(outer * rows, conv_width)
-    sums = jnp.stack([jnp.sum(filtered, axis=-1), jnp.sum(filtered * filtered, axis=-1)])
-
-    state_mixed, totals = states(
-        pair, sums, local, carried, quarter(per_head_norm_gain)[None], head_size, "sp", "tp"
-    )
-    conv_channels = conv_width * outer * lax.axis_size("tp")
-    row_mean = totals[0] / conv_channels
-    deviation = filtered - row_mean[:, None]
-    variance = totals[1] / conv_channels - row_mean * row_mean
-    conv_mixed = jax.nn.silu(
-        deviation * lax.rsqrt(variance + LAYER_EPSILON)[:, None] * quarter(convolution_channel_gain)
-    ).astype(jnp.bfloat16)
-    return reduce_rows(state_mixed, conv_mixed, both_out, outer, "sp", "tp")
 
 
 def solution(mesh):

time: 193 us -> 155 us (0.80)
  Pallas kernels: 170 us -> 150 us
  other arithmetic: 8.98 us -> 1.3 us
  matrix products: 5.15 us -> 0 us
  local copies, waits for them, and re-layouts: 6.52 us -> 3 us
    pallas_call x2 -> x0, Pallas kernels: 67.9 us -> none  [the longest x1 47.5 us: reduce_rows(): pl.pallas_call(functools.partial(reduce_kernel, axis, pair_axis, radices)...]
    pallas_call x1, Pallas kernels: 102 us -> 150 us  [spread(): pl.pallas_call(functools.partial(spread_kernel, axis, pair_axis, radices,...]
    dot_general x2 -> x0, matrix products: 5.15 us -> none  [the longest x1 3.9 us: fast_body(): jnp.dot(normed, conv_in[:, conv_width:], preferred_element_type=jnp.float32)]
    reduce_sum x1 -> x0, other arithmetic: 5.06 us -> none  [fast_body(): jnp.sum(filtered, axis=-1)]
    slice x4 -> x0, local copies, waits for them, and re-layouts: 2.35 us -> none  [the longest x2 2.32 us: fast_body(): filtered = filtered + taps[offset] * padded[:, offset:offset + rows]]
  transfers between devices with their start and end apart: 1 -> 0, of which waited for: 0 -> 0; matrix products, arithmetic and copies ran while one was open for 2% -> 0% of each run, Pallas kernels for 0% -> 0%
where the time goes in v3:
time: 155 us; the launch traced here: 154 us
  Pallas kernels  150 us (97%)
  local copies, waits for them, and re-layouts  3 us (2%)
    pallas_call x1, Pallas kernels, spread(): pl.pallas_call(functools.partial(spread_kernel, axis, pair_axis, radices,...  150 us

profile of v3, /device:TPU:0, one launch (start us, length us, event | category | flops | bytes accessed | tf_op | source)
XLA Modules:
  0.0 154.3 jit_solution(4436304001056450270)
XLA Ops:
  0.0 0.0 copy-start
  0.0 0.7 copy-done
  0.7 1.3 pad_maximum_fusion.refs_2_
  2.0 150.0 %whole_layer.1 = bf16[256,2048]{1,0:T(8,128)(2,1)} custom-call(bf16[256,2048]{1,0:T(8,128)(2,1)} %refs_0_.1, f32[1,2048]{1,0:T(1,128)} %bitcast.9, f32[16,256]{1,0:T(8,128)} %pad_maximum_fusion.refs_2_, bf16[128,512]{1,0:T(8,128)(2,1)} %refs_3_.1, bf16[128,512]{1,0:T(8,128)(2,1)} %refs_4_.1, bf16[128,512]{1,0:T(8,128)(2,1)} %refs_5_.1, ...), custom_call_target="tpu_custom_call" | custom-call | flops 10000000000 | bytes 16777216 | tf_op jit(solution)/shard_map/whole_layer/pallas_call | solution.py:789
  152.0 2.3 %copy.22 = bf16[256,2048]{1,0:T(8,128)(2,1)} copy(bf16[256,2048]{1,0:T(8,128)(2,1)} %whole_layer.1) | data formatting | bytes 2097152
Async XLA Ops:
  0.0 0.7 copy-start

commit v4 on v3

--- a/solution.py
+++ b/solution.py
@@ -423,10 +423,12 @@
     return me // (inner * middle), (me // inner) % middle, me % inner
 
 
-def greet(devices):
+def greet(devices, meanwhile=None):
     barrier = pltpu.get_barrier_semaphore()
     for device in devices:
         pl.semaphore_signal(barrier, inc=1, device_id=device, device_id_type=MESH)
+    if meanwhile is not None:
+        meanwhile()
     pl.semaphore_wait(barrier, len(devices))
 
 
@@ -446,9 +448,6 @@
     outer, middle, inner = radices
     z, y, x = place_of(axis, radices)
     core = lax.axis_index(pair_axis)
-    widened = raw_ref[...].astype(jnp.float32)
-    scale = lax.rsqrt(jnp.mean(widened * widened, axis=-1, keepdims=True) + RMS_EPSILON)
-    tokens_ref[...] = (widened * scale * gain_ref[...]).astype(jnp.bfloat16)
     half = tokens_ref.shape[0] // 2
     mine, other = pl.ds(pl.multiple_of(core * half, half), half), pl.ds(pl.multiple_of((1 - core) * half, half), half)
 
@@ -464,7 +463,13 @@
         pair_ref, stats_ref, local_ref, carried_ref, head_gain_ref, filtered_ref, conv_gain_ref, last_out, out_ref,
         *finish_refs,
     )
-    greet(peers)
+
+    def normalize():
+        widened = raw_ref[...].astype(jnp.float32)
+        scale = lax.rsqrt(jnp.mean(widened * widened, axis=-1, keepdims=True) + RMS_EPSILON)
+        tokens_ref[...] = (widened * scale * gain_ref[...]).astype(jnp.bfloat16)
+
+    greet(peers, normalize)
 
     def part(w, at):
         return ins[w].at[:, pl.ds(pl.multiple_of(at * widths[w], widths[w]), widths[w])]
@@ -612,8 +617,6 @@
         side_copy(step, far[step], (z + outer - step - 1) % outer).wait_recv()
     token_step(0)
     send_far(rest[1])
-    for w in rest[0]:
-        advance(w, 0)
     one_block, chain, read = delta_phases(
         z, head_size, chunk, block, proj, side_out, decay_ref, rate_ref, decay_offset_ref, rate_offset_ref,
         local_ref, carried_ref, pair_ref, mats, adds, hist, queries,
@@ -634,51 +637,16 @@
             total = term if total is None else total + term
         proj[...] = total
 
-    def one_round(k, carry):
+    conv_width = second_out.shape[-1] // 2
+    rows, rim_rows = tokens_ref.shape[0], rim_out.shape[1]
+
+    def group_of(k):
         twosided = k <= 2 * edge
         distance = jnp.where(twosided, (k + 1) // 2, k - edge)
-        side = jnp.where(twosided & (k % 2 == 1), toward, -toward)
-        group = z + side * distance
-
-        @pl.when(k > 0)
-        def _():
-            sibling_step(k - 1)
-
-        project(group)
-        for piece in range(pieces):
-            one_block(group, piece)
-            if piece == 0:
-                @pl.when(k == 0)
-                def _():
-                    for w in rest[0]:
-                        advance(w, 1)
-
-                @pl.when(k == 2)
-                def _():
-                    for w in rest[1]:
-                        advance(w, 1)
-
-                @pl.when((k > 0) & (k < outer - 1))
-                def _():
-                    token_step(k)
-
-                @pl.when(k == 1)
-                def _():
-                    for w in rest[1]:
-                        advance(w, 0)
-        return carry
-
-    lax.fori_loop(0, outer, one_round, 0)
-    chain()
-
-    rows = tokens_ref.shape[0]
-    span, rim_rows = taps_ref.shape[0], rim_out.shape[1]
-    conv_width = second_out.shape[-1] // 2
-    for w in rest[0]:
-        advance(w, last)
-
-    def gate(group, carry):
-        total = None
+        return z + jnp.where(twosided & (k % 2 == 1), toward, -toward) * distance
+
+    def gate(k, carry):
+        group, total = group_of(k), None
         for part_at in range(outer):
             matrix = second_out[part_at].reshape(piece_depth, 2 * conv_width)
             term = jnp.dot(
@@ -691,12 +659,53 @@
         rim_out[group] = gated[rows - rim_rows :]
         return carry
 
-    lax.fori_loop(0, outer, gate, 0)
+    def one_round(k, carry):
+        group = group_of(k)
+
+        @pl.when(k == outer - 1)
+        def _():
+            for w in rest[1]:
+                advance(w, 0)
+            for w in rest[0]:
+                advance(w, last)
+            lax.fori_loop(0, outer - 1, gate, 0)
+            for w in rest[1]:
+                advance(w, 1)
+            token_step(outer - 2)
+
+        @pl.when(k > 0)
+        def _():
+            sibling_step(k - 1)
+
+        project(group)
+        for piece in range(pieces):
+            one_block(group, piece)
+            if piece == 0:
+                @pl.when(k == 1)
+                def _():
+                    for w in rest[0]:
+                        advance(w, 1)
+
+                @pl.when((k > 0) & (k < outer - 2))
+                def _():
+                    token_step(k)
+
+        @pl.when(k == 0)
+        def _():
+            for w in rest[0]:
+                advance(w, 0)
+
+        return carry
+
+    lax.fori_loop(0, outer, one_round, 0)
+    gate(outer - 1, 0)
+    span = taps_ref.shape[0]
     rim_copy = pltpu.make_async_remote_copy(
         src_ref=rim_out, dst_ref=rim_in, send_sem=rim_send.at[0], recv_sem=rim_recv.at[0],
         device_id={axis: z * planes + (plane + 1) % planes}, device_id_type=MESH,
     )
     rim_copy.start()
+    chain()
     send_pairs()
     read()
     rim_copy.wait_recv()

time: 155 us -> 151 us (0.974)
  Pallas kernels: 150 us -> 146 us
    pallas_call x1, Pallas kernels: 150 us -> 146 us  [spread(): pl.pallas_call(functools.partial(spread_kernel, axis, pair_axis, radices,...]
where the time goes in v4:
time: 151 us; the launch traced here: 150 us
  Pallas kernels  146 us (97%)
  local copies, waits for them, and re-layouts  3 us (2%)
    pallas_call x1, Pallas kernels, spread(): pl.pallas_call(functools.partial(spread_kernel, axis, pair_axis, radices,...  146 us

profile of v4, /device:TPU:0, one launch (start us, length us, event | category | flops | bytes accessed | tf_op | source)
XLA Modules:
  0.0 150.4 jit_solution(4644876276097836112)
XLA Ops:
  0.0 0.0 copy-start
  0.0 0.7 copy-done
  0.7 1.3 pad_maximum_fusion.refs_2_
  2.0 146.0 %whole_layer.1 = bf16[256,2048]{1,0:T(8,128)(2,1)} custom-call(bf16[256,2048]{1,0:T(8,128)(2,1)} %refs_0_.1, f32[1,2048]{1,0:T(1,128)} %bitcast.9, f32[16,256]{1,0:T(8,128)} %pad_maximum_fusion.refs_2_, bf16[128,512]{1,0:T(8,128)(2,1)} %refs_3_.1, bf16[128,512]{1,0:T(8,128)(2,1)} %refs_4_.1, bf16[128,512]{1,0:T(8,128)(2,1)} %refs_5_.1, ...), custom_call_target="tpu_custom_call" | custom-call | flops 10000000000 | bytes 16777216 | tf_op jit(solution)/shard_map/whole_layer/pallas_call | solution.py:798
  148.1 2.3 %copy.22 = bf16[256,2048]{1,0:T(8,128)(2,1)} copy(bf16[256,2048]{1,0:T(8,128)(2,1)} %whole_layer.1) | data formatting | bytes 2097152
Async XLA Ops:
  0.0 0.7 copy-start
